TPU v7x, 256 devices: a 4x2x16 block of a 4x16x16 slice. The times are simulated.
256 devices in a mesh: grp: 2 (over y), sp: 16 (over z), fs: 4 (over x), tp: 2 (over core).
Axes of the slice: x: 4, y: 2, z: 16, core: 2. Of those that a mesh axis runs over, the one named last changes fastest.
The devices are a block of a 4x16x16 slice.
Arguments:
- tokens: bfloat16 [16, 1024, 2048], P(('grp', 'fs'), 'sp'), parts along dimension 0, may hold values from -6 to 6
- pre_gain: float32 [2048], replicated, may hold values from 0.1 to 1.9
- query_weight: bfloat16 [2048, 1024], P(('sp', 'fs'), 'tp'), may hold values from -0.125 to 0.125
- key_weight: bfloat16 [2048, 1024], P(('sp', 'fs'), 'tp'), may hold values from -0.125 to 0.125
- value_weight: bfloat16 [2048, 1024], P(('sp', 'fs'), 'tp'), may hold values from -0.125 to 0.125
- beta_weight: bfloat16 [2048, 8], replicated, may hold values from -0.125 to 0.125
- decay_weight: bfloat16 [2048, 8], replicated, may hold values from -0.125 to 0.125
- decay_rate: float32 [8], replicated, may hold values from 0 to 1
- delta_gain: float32 [128], replicated, may hold values from 0.1 to 1.9
- query_down: bfloat16 [2048, 512], P(('sp', 'fs')), may hold values from -0.125 to 0.125
- latent_down: bfloat16 [2048, 256], P(('sp', 'fs')), may hold values from -0.125 to 0.125
- rope_weight: bfloat16 [2048, 32], replicated, may hold values from -0.125 to 0.125
- query_gain: float32 [512], replicated, may hold values from 0.1 to 1.9
- latent_gain: float32 [256], replicated, may hold values from 0.1 to 1.9
- query_up: bfloat16 [512, 1536], P(None, 'tp'), may hold values from -4 to 4
- latent_up: bfloat16 [256, 2048], P(None, 'tp'), may hold values from -4 to 4
- delta_out: bfloat16 [1024, 2048], P('tp', ('sp', 'fs')), may hold values from -8 to 8
- latent_out: bfloat16 [1024, 2048], P('tp', ('sp', 'fs')), may hold values from -8 to 8
- post_gain: float32 [2048], P('tp'), may hold values from 0.1 to 1.9
Outputs:
- mixed_out: bfloat16 [16, 1024, 2048], P(('grp', 'fs'), 'sp', 'tp'), parts along dimension 0
There are 2 independent parts, one for each index of `grp`. A program takes and returns all parts, laid end to end along the dimension named above; an argument that names none is the same for every part. Nothing has to cross between parts.
All inputs are finite; a program needn't handle non-finite values.
Results may differ from a plain program's by a relative error of at most 0.018.
The roundings to bfloat16 on the way count: a program that leaves them out, or rounds other values in their place, can miss the bound.
Values may be sent and summed in bfloat16 or wider, within the bound.
A program may use at most 128 MiB of HBM per device.

v0:
```python
import math

import jax
import jax.numpy as jnp
from jax import lax
from jax.sharding import PartitionSpec as P

HEAD = 128
NOPE = 64
ROPE = 32
VDIM = 64
BLOCK = 64


NORM_EPS = 1e-06
ROPE_THETA = 10000.0
HIGHEST = lax.Precision.HIGHEST


def sent_together(arrays, axis, dim, along):
    widths = [a.shape[along] for a in arrays]
    both = jnp.concatenate(arrays, axis=along)
    filled = lax.all_gather(both, axis, axis=dim, tiled=True)
    return tuple(jnp.split(filled, [sum(widths[:k]) for k in range(1, len(widths))], axis=along))


def joined_along(tiles, dim):
    shape = list(tiles.shape[1:])
    shape[dim] *= tiles.shape[0]
    return jnp.moveaxis(tiles, 0, dim).reshape(shape)


def one_gather(arrays, axis, dims):
    vector = jnp.concatenate([a.reshape(-1) for a in arrays])
    lines, at, done = (lax.all_gather(vector, axis), 0, [])
    for a, dim in zip(arrays, dims):
        tiles = lines[:, at : at + a.size].reshape(-1, *a.shape)
        done.append(joined_along(tiles, dim))
        at += a.size
    return tuple(done)


def prefix(array, axis, join, neutral):
    place = lax.axis_index(axis)
    gathered = jax.tree.map(
        lambda a, kind: lax.all_gather(a.astype(kind), axis), array, (jnp.bfloat16, jnp.bfloat16)
    )
    state = jax.tree.map(lambda a, e: jnp.zeros_like(a) + jnp.asarray(e, a.dtype), array, neutral)

    def one(step, state):
        return join(
            state,
            jax.tree.map(
                lambda a, own: lax.dynamic_index_in_dim(a, step, 0, False).astype(own.dtype),
                gathered,
                array,
            ),
        )

    return lax.fori_loop(0, place, one, state)


def gather_axes(array, axes, dim):
    if not axes:
        return array
    nearer = lax.all_gather(array, axes[-1], axis=dim, tiled=True)
    return gather_axes(nearer, axes[:-1], dim)


def copy_for_each(array, axis):
    devices = lax.axis_size(axis)
    return lax.all_to_all(
        jnp.broadcast_to(array[None], (devices, *array.shape)), axis, 0, 0, tiled=True
    )


def taken_together(array, axis):
    return copy_for_each(array, axis).astype(jnp.float32).sum(axis=0)


def stored(values):
    return lax.optimization_barrier(values.astype(jnp.bfloat16))


def rms_scale(values):
    return lax.rsqrt(jnp.mean(values * values, axis=-1, keepdims=True) + NORM_EPS)


def unit_rows(values):
    return values * lax.rsqrt(jnp.sum(values * values, axis=-1, keepdims=True) + NORM_EPS)


def rope_tables(positions, rope_width):
    frequency = ROPE_THETA ** (-jnp.arange(0, rope_width, 2, dtype=jnp.float32) / rope_width)
    angles = positions.astype(jnp.float32)[:, None] * frequency[None, :]
    return (jnp.cos(angles), jnp.sin(angles))


def rotate(values, cosine_table, sine_table):
    lower_half, upper_half = jnp.split(values, 2, axis=-1)
    return jnp.concatenate(
        [
            lower_half * cosine_table - upper_half * sine_table,
            upper_half * cosine_table + lower_half * sine_table,
        ],
        axis=-1,
    )


def delta_terms(query_vectors, key_vectors, value_vectors, beta_gate, log_decay):
    length, head_count, head_width = query_vectors.shape
    nblocks = length // BLOCK

    def split_blocks(tensor):
        return jnp.moveaxis(tensor.reshape((nblocks, BLOCK, head_count) + tensor.shape[2:]), 2, 0)

    query_vectors = split_blocks(query_vectors)
    key_vectors = split_blocks(key_vectors)
    value_vectors = split_blocks(value_vectors)
    beta_gate = split_blocks(beta_gate)
    gate_sum = jnp.cumsum(split_blocks(log_decay), axis=-1)
    position = jnp.arange(BLOCK)
    strict = position[:, None] > position[None, :]
    causal = position[:, None] >= position[None, :]
    gate_gap = gate_sum[..., :, None] - gate_sum[..., None, :]
    strict_decay = jnp.where(strict, jnp.exp(jnp.where(strict, gate_gap, 0.0)), 0.0)
    causal_decay = jnp.where(causal, jnp.exp(jnp.where(causal, gate_gap, 0.0)), 0.0)
    keys_scaled = key_vectors * beta_gate[..., None]
    lower_mat = (
        jnp.einsum("hnid,hnjd->hnij", keys_scaled, key_vectors, precision=HIGHEST) * strict_decay
    )
    identity = jnp.eye(BLOCK, dtype=jnp.float32)
    inverse = jax.scipy.linalg.solve_triangular(
        identity + lower_mat, jnp.broadcast_to(identity, lower_mat.shape), lower=True
    )
    new_values = jnp.einsum(
        "hnij,hnjd->hnid", inverse, value_vectors * beta_gate[..., None], precision=HIGHEST
    )
    key_weights = jnp.einsum(
        "hnij,hnjd->hnid", inverse, keys_scaled * jnp.exp(gate_sum)[..., None], precision=HIGHEST
    )
    scores = (
        jnp.einsum("hnid,hnjd->hnij", query_vectors, key_vectors, precision=HIGHEST) * causal_decay
    )
    last_gate = gate_sum[..., -1]
    query_decay = query_vectors * jnp.exp(gate_sum)[..., None]
    key_decay = key_vectors * jnp.exp(last_gate[..., None] - gate_sum)[..., None]
    return (query_decay, key_decay, new_values, key_weights, scores, last_gate)


def compose(earlier, following):
    return (
        jnp.einsum("hij,hjk->hik", following[0], earlier[0], precision=HIGHEST),
        jnp.einsum("hij,hjk->hik", following[0], earlier[1], precision=HIGHEST) + following[1],
    )


def keep_same(current):
    return current


def local(
    tokens,
    pre_gain,
    query_weight,
    key_weight,
    value_weight,
    beta_weight,
    decay_weight,
    decay_rate,
    delta_gain,
    query_down,
    latent_down,
    rope_weight,
    query_gain,
    latent_gain,
    query_up,
    latent_up,
    delta_out,
    latent_out,
    post_gain,
):
    f32 = jnp.float32
    seq_count, token_count = (tokens.shape[0], tokens.shape[1])
    row_total = seq_count * token_count
    sequence = tokens.reshape(row_total, tokens.shape[2]).astype(f32)
    query_start = lax.axis_index("sp") * token_count
    positions = query_start + jnp.arange(token_count)
    normed = (sequence * rms_scale(sequence) * pre_gain).astype(jnp.bfloat16)
    head_group = lax.axis_index("tp")
    q_width = query_down.shape[1] // lax.axis_size("tp")
    kv_width = latent_down.shape[1] // lax.axis_size("tp")
    q_own = lax.dynamic_slice_in_dim(query_down, head_group * q_width, q_width, 1)
    kv_own = lax.dynamic_slice_in_dim(latent_down, head_group * kv_width, kv_width, 1)
    weights = (query_weight, key_weight, value_weight, q_own, kv_own)
    portion = sent_together(
        (query_weight, key_weight, value_weight, q_own, kv_own), ("sp", "fs"), 0, 1
    )
    row_count = portion[0].shape[0]
    projected = tuple((jnp.dot(normed, weight, preferred_element_type=f32) for weight in portion))
    raw_query, raw_key, raw_value, q_half, kv_half = tuple((stored(member) for member in projected))
    q_latent, kv_latent = one_gather((q_half, kv_half), "tp", (1, 1))
    head_count = query_weight.shape[1] // HEAD
    lane_count = seq_count * head_count
    beta_full = jax.nn.sigmoid(jnp.dot(normed, beta_weight, preferred_element_type=f32))
    beta_gate = lax.dynamic_slice_in_dim(beta_full, head_group * head_count, head_count, 1)
    decay_full = jnp.dot(normed, decay_weight, preferred_element_type=f32)
    decay_pre = lax.dynamic_slice_in_dim(decay_full, head_group * head_count, head_count, 1)
    decay_local = lax.dynamic_slice_in_dim(decay_rate, head_group * head_count, head_count, 0)
    log_decay = -decay_local[None, :] * jax.nn.softplus(decay_pre)

    def by_position(values):
        shaped = values.reshape((seq_count, token_count) + values.shape[1:])
        shaped = jnp.moveaxis(shaped, 0, 1)
        return shaped.reshape((token_count, seq_count * values.shape[1]) + values.shape[2:])

    query_vectors = by_position(
        unit_rows(jax.nn.silu(raw_query.astype(f32)).reshape(row_total, head_count, HEAD))
        * HEAD ** (-0.5)
    )
    key_vectors = by_position(
        unit_rows(jax.nn.silu(raw_key.astype(f32)).reshape(row_total, head_count, HEAD))
    )
    value_vectors = by_position(
        jax.nn.silu(raw_value.astype(f32)).reshape(row_total, head_count, HEAD)
    )
    block_terms = delta_terms(
        query_vectors, key_vectors, value_vectors, by_position(beta_gate), by_position(log_decay)
    )
    inputs = tuple((jnp.moveaxis(tensor, 1, 0) for tensor in block_terms))

    def advance(totals, block_in):
        carried, transfer = totals
        query_decay, key_decay, new_values, key_weights, scores, last_gate = block_in
        corrected = new_values - jnp.einsum("hcd,hde->hce", key_weights, carried, precision=HIGHEST)
        output = jnp.einsum("hcd,hde->hce", query_decay, carried, precision=HIGHEST) + jnp.einsum(
            "hij,hje->hie", scores, corrected, precision=HIGHEST
        )
        reader_rows = query_decay - jnp.einsum(
            "hij,hjd->hid", scores, key_weights, precision=HIGHEST
        )
        reader = jnp.einsum("hcd,hde->hce", reader_rows, transfer, precision=HIGHEST)
        factor = jnp.exp(last_gate)[:, None, None]
        carried = carried * factor + jnp.einsum(
            "hcd,hce->hde", key_decay, corrected, precision=HIGHEST
        )
        moved = jnp.einsum("hcd,hde->hce", key_weights, transfer, precision=HIGHEST)
        transfer = transfer * factor - jnp.einsum(
            "hcd,hce->hde", key_decay, moved, precision=HIGHEST
        )
        return ((carried, transfer), (output, reader))

    eye_stack = jnp.broadcast_to(jnp.eye(HEAD, dtype=f32), (lane_count, HEAD, HEAD))
    zero_state = jnp.zeros((lane_count, HEAD, HEAD), f32)
    (state_end, transfer_end), (outputs, readers) = lax.scan(
        advance, (zero_state, eye_stack), inputs
    )
    _, incoming = prefix((transfer_end, state_end), "sp", compose, (eye_stack, zero_state))
    outputs = outputs + jnp.einsum("nhcd,hde->nhce", readers, incoming, precision=HIGHEST)
    delta_raw = jnp.transpose(outputs, (0, 2, 1, 3)).reshape(
        token_count, seq_count, head_count, HEAD
    )
    delta_raw = jnp.moveaxis(delta_raw, 1, 0).reshape(row_total, head_count, HEAD)
    delta_heads = (
        (delta_raw * rms_scale(delta_raw) * delta_gain)
        .astype(jnp.bfloat16)
        .reshape(row_total, head_count * HEAD)
    )
    q_lat32 = q_latent.astype(f32)
    kv_lat32 = kv_latent.astype(f32)
    q_normed = (q_lat32 * rms_scale(q_lat32) * query_gain).astype(jnp.bfloat16)
    kv_normed = (kv_lat32 * rms_scale(kv_lat32) * latent_gain).astype(jnp.bfloat16)
    rope_raw = stored(jnp.dot(normed, rope_weight, preferred_element_type=f32))
    cosine_table, sine_table = rope_tables(positions, rope_raw.shape[1])
    rope_keys = rotate(
        rope_raw.astype(f32).reshape(seq_count, token_count, rope_raw.shape[1]),
        cosine_table,
        sine_table,
    ).astype(jnp.bfloat16)
    latent_count = query_up.shape[1] // (NOPE + ROPE)
    query_all = stored(jnp.dot(q_normed, query_up, preferred_element_type=f32)).reshape(
        seq_count, token_count, latent_count, NOPE + ROPE
    )
    query_plain = query_all[..., :NOPE]
    query_turned = rotate(
        query_all[..., NOPE:].astype(f32), cosine_table[:, None, :], sine_table[:, None, :]
    ).astype(jnp.bfloat16)
    score_scale = (NOPE + ROPE) ** (-0.5)
    query_block = positions // BLOCK
    kv_seq = kv_normed.reshape(seq_count, token_count, kv_normed.shape[1])

    def attend_block(totals, key_plain, value_rows, rope_rows, key_start):
        row_max, row_sum, weighted = totals
        key_block = (key_start + jnp.arange(key_plain.shape[1])) // BLOCK
        allowed = key_block[None, :] <= query_block[:, None]
        logits = (
            jnp.einsum("sqhd,skhd->shqk", query_plain, key_plain, preferred_element_type=f32)
            + jnp.einsum("sqhd,skd->shqk", query_turned, rope_rows, preferred_element_type=f32)
        ) * score_scale
        logits = jnp.where(allowed[None, None], logits, -jnp.inf)
        new_max = jnp.maximum(row_max, jnp.max(logits, axis=-1))
        shift = jnp.where(jnp.isfinite(new_max), new_max, 0.0)
        weights = jnp.where(allowed[None, None], jnp.exp(logits - shift[..., None]), 0.0)
        rescale = jnp.exp(row_max - shift)
        row_sum = row_sum * rescale + jnp.sum(weights, axis=-1)
        weighted = weighted * rescale[..., None] + jnp.einsum(
            "shqk,skhd->shqd", weights.astype(jnp.bfloat16), value_rows, preferred_element_type=f32
        )
        return (new_max, row_sum, weighted)

    start_stats = (
        jnp.full((seq_count, latent_count, token_count), -jnp.inf, f32),
        jnp.zeros((seq_count, latent_count, token_count), f32),
        jnp.zeros((seq_count, latent_count, token_count, VDIM), f32),
    )

    def expand_latent(portion, row_start, span_rows):
        latent_rows = lax.dynamic_slice_in_dim(portion[0], row_start, span_rows, 1)
        expanded = jnp.dot(
            latent_rows.reshape(seq_count * span_rows, latent_rows.shape[2]),
            latent_up,
            preferred_element_type=f32,
        ).astype(jnp.bfloat16)
        expanded = expanded.reshape(seq_count, span_rows, latent_count, NOPE + VDIM)
        return (
            expanded[..., :NOPE],
            expanded[..., NOPE:],
            lax.dynamic_slice_in_dim(portion[1], row_start, span_rows, 1),
        )

    portion = sent_together((kv_seq, rope_keys), "sp", 1, 2)
    row_count = portion[0].shape[1]
    span_rows = math.gcd(row_count, token_count * max(1, 512 // token_count))

    def visit_rows(current):

        def visit_block(block_index, stats):
            row_start = block_index * span_rows
            key_plain, value_rows, rope_rows = expand_latent(portion, row_start, span_rows)
            return attend_block(stats, key_plain, value_rows, rope_rows, row_start)

        return lax.fori_loop(0, row_count // span_rows, visit_block, current)

    row_max, row_sum, weighted = lax.cond(
        jnp.int32(0) < query_start + token_count, visit_rows, keep_same, start_stats
    )
    latent_heads = (
        jnp.transpose(weighted / row_sum[..., None], (0, 2, 1, 3))
        .reshape(row_total, latent_count * VDIM)
        .astype(jnp.bfloat16)
    )
    heads_joined = jnp.concatenate([delta_heads, latent_heads], axis=1)
    out_rows = jnp.concatenate([delta_out, latent_out], axis=0)
    partial_value = jnp.dot(
        heads_joined, gather_axes(out_rows, ("sp", "fs"), 1), preferred_element_type=f32
    )
    whole_rows = taken_together(partial_value.astype(jnp.bfloat16), "tp").astype(jnp.float32)
    row_scale = rms_scale(whole_rows)
    half_width = post_gain.shape[0]
    own_half = lax.dynamic_slice_in_dim(whole_rows, head_group * half_width, half_width, 1)
    result = own_half * row_scale * post_gain
    return result.astype(jnp.bfloat16).reshape(seq_count, token_count, result.shape[1])


def solution(mesh):
    return jax.shard_map(
        local,
        mesh=mesh,
        in_specs=(
            P(("grp", "fs"), "sp", None),
            P(),
            P(("sp", "fs"), "tp"),
            P(("sp", "fs"), "tp"),
            P(("sp", "fs"), "tp"),
            P(),
            P(),
            P(),
            P(),
            P(("sp", "fs"), None),
            P(("sp", "fs"), None),
            P(),
            P(),
            P(),
            P(None, "tp"),
            P(None, "tp"),
            P("tp", ("sp", "fs")),
            P("tp", ("sp", "fs")),
            P("tp"),
        ),
        out_specs=P(("grp", "fs"), "sp", "tp"),
        check_vma=False,
    )
```

profile of v0, /device:TPU:33, one launch (start us, length us, event | category | flops | bytes accessed | tf_op | source)
XLA Modules:
  0.0 490.5 jit_solution(5723787358120266488)
XLA Ops:
  6.6 0.8 constant_dynamic-update-slice_fusion.3
  7.5 0.8 constant_dynamic-update-slice_fusion.2
  8.2 0.8 constant_dynamic-update-slice_fusion.1
  9.0 0.7 dynamic-slice_dynamic-update-slice_fusion
  9.7 0.7 constant_dynamic-update-slice_fusion
  10.4 0.6 copy-done.3
  11.2 1.2 multiply_reduce_fusion.1
  12.8 0.7 dynamic-slice_negate_fusion
  13.6 1.2 fusion.53
  16.7 152.6 %all-gather.9.cloned.1.call-done = bf16[2048,1920]{1,0:T(8,128)(2,1)} async-done(((bf16[32,1920]{1,0:T(8,128)(2,1)}), bf16[2048,1920]{1,0:T(8,128)(2,1)}) %all-gather.9.cloned.1.call-update) | async-done | bytes 7864336 | tf_op jit(solution)/shard_map/all_gather | solution.py:23
  169.2 1.3 convolution_convert_fusion.3
  170.5 1.5 convolution_convert_fusion.2
  172.2 10.2 %all-gather.2 = bf16[98304]{0:T(1024)(128)(2,1)S(1)} all-gather(bf16[49152]{0:T(1024)(128)(2,1)S(1)} %pad_maximum_fusion.1), channel_id=4, replica_groups=mesh['grp'=2,'sp'=16,'fs'=4,'tp'=2] {'tp'}, dimensions={0}, use_global_device_ids=true | all-gather | bytes 294912 | tf_op jit(solution)/shard_map/all_gather | solution.py:35
  183.1 0.7 pad_maximum_fusion.2
  184.0 2.0 fusion.45
  186.0 2.0 fusion.42
  189.8 39.3 %custom-call.4 = f32[8,1,64,64]{2,3,1,0:T(8,128)S(1)} custom-call(f32[8,1,64,64]{3,2,1,0:T(8,128)S(1)} %fusion.37), custom_call_target="InvertDiagBlocksLowerTriangular" | custom-call | tf_op jit(solution)/shard_map/jit(_solve_triangular)/vmap()/triangular_solve | solution.py:133
  230.8 1.8 fusion.32
  233.5 1.8 fusion.33
  235.4 10.6 %all_gather.38 = bf16[1024,128]{0,1:T(8,128)(2,1)} all-gather(bf16[1024,32]{0,1:T(8,128)(2,1)S(1)} %pad_maximum_fusion.3), channel_id=1, replica_groups=mesh['grp'=2,'sp'=16,'fs'=4,'tp'=2] {'fs'}, dimensions={1}, use_global_device_ids=true | all-gather | bytes 327680 | tf_op jit(solution)/shard_map/all_gather | solution.py:66
  247.7 2.0 fusion.39
  252.0 1.1 fusion.34
  254.1 20.1 %conditional.1 = (f32[2,8,64]{2,1,0:T(8,128)}, f32[2,8,64,64]{3,2,1,0:T(8,128)}) conditional(s32[]{:T(128)} %convert_element_type.188, () %tuple.64, (bf16[2,1024,288]{2,1,0:T(8,128)(2,1)}, s32[64]{0:T(128)S(1)}, s32[64]{0:T(128)S(1)}, s32[]{:T(128)}, bf16[2,64,8,96]{3,2,1,0:T(8,128)(2,1)S(1)}, /*index=5*/bf16[256,1024]{1,0:T(8,128)(2,1)S(1)}, ...), branch_computations={%region_11.12_spmd, %region_12.17_spmd.clone} | conditional | flops 711182272 | bytes 31335772 | solution.py:344
  254.2 1.3 split.52
  255.5 2.5 copy.128
  258.0 0.9 split.54
  258.9 15.3 %while.51 = (s32[]{:T(128)}, f32[2,8,64]{2,1,0:T(8,128)S(1)}, f32[2,8,64]{2,1,0:T(8,128)}, f32[2,8,64,64]{3,2,1,0:T(8,128)}, s32[64]{0:T(128)S(1)}, /*index=5*/b...) while((s32[]{:T(128)}, f32[2,8,64]{2,1,0:T(8,128)S(1)}, ...), condition=%wide.region_16.16_spmd.clone, body=%wide.region_13.15_spmd.clone.sunk | while | flops 711181312 | bytes 26223056 | solution.py:342
  259.1 0.7 convert_bitcast_fusion.3
  260.4 0.7 fusion.169
  261.1 0.9 fusion.170
  262.0 0.6 fusion.171
  262.6 0.7 fusion.172
  263.3 0.6 fusion.173
  263.9 1.7 fusion.174
  265.8 0.7 convert_bitcast_fusion.3
  267.2 0.7 fusion.169
  267.9 0.9 fusion.170
  269.4 0.7 fusion.172
  270.1 1.3 fusion.173
  271.4 2.8 fusion.174
  274.2 1.3 fusion.94
  275.9 39.6 %all-gather.15.cloned.1.call-done = bf16[128,128,128]{2,1,0:T(8,128)(2,1)} async-done(((bf16[8,128,128]{2,1,0:T(8,128)(2,1)}), bf16[128,128,128]{2,1,0:T(8,128)(2,1)}) %all-gather.15.cloned.1.call-update) | async-done | bytes 4194320 | tf_op jit(solution)/shard_map/all_gather | solution.py:46
  315.4 74.7 %all-gather.17.cloned.1.call-done = bf16[128,128,128]{2,1,0:T(8,128)(2,1)} async-done(((bf16[8,128,128]{2,1,0:T(8,128)(2,1)}), bf16[128,128,128]{2,1,0:T(8,128)(2,1)}) %all-gather.17.cloned.1.call-update) | async-done | bytes 4194320 | tf_op jit(solution)/shard_map/all_gather | solution.py:46
  390.4 0.7 copy-done.2
  392.4 72.3 %all-gather.13.cloned.1.call-done = bf16[1024,2048]{0,1:T(8,128)(2,1)} async-done(((bf16[1024,128]{0,1:T(8,128)(2,1)}), bf16[1024,2048]{0,1:T(8,128)(2,1)}) %all-gather.13.cloned.1.call-update) | async-done | bytes 4194320 | tf_op jit(solution)/shard_map/all_gather | solution.py:66
  464.7 3.7 convolution_convert_fusion
  468.6 13.9 %all_to_all.5 = bf16[2,128,2048]{2,1,0:T(8,128)(2,1)S(1)} all-to-all(bf16[2,128,2048]{2,1,0:T(8,128)(2,1)S(1)} %broadcast_in_dim.191), channel_id=1, replica_groups=mesh['grp'=2,'sp'=16,'fs'=4,'tp'=2] {'tp'}, dimensions={0} | all-to-all | bytes 2097152 | tf_op jit(solution)/shard_map/all_to_all | solution.py:72
  483.1 0.8 multiply_convert_fusion
  (148 shorter events, 17.0 us)
Async XLA Ops:
  6.5 240.5 %copy-start = (bf16[512,768]{1,0:T(8,128)(2,1)S(1)}, bf16[512,768]{1,0:T(8,128)(2,1)}, u32[]{:S(2)}) copy-start(bf16[512,768]{1,0:T(8,128)(2,1)} %param.39) | copy-start | bytes 2359300
  6.6 8.3 %copy-start.5 = (bf16[2048,8]{0,1:T(8,128)(2,1)S(1)}, bf16[2048,8]{0,1:T(8,128)(2,1)}, u32[]{:S(2)}) copy-start(bf16[2048,8]{0,1:T(8,128)(2,1)} %param.30) | copy-start | bytes 98308
  6.6 8.5 %copy-start.6 = (bf16[2048,8]{0,1:T(8,128)(2,1)S(1)}, bf16[2048,8]{0,1:T(8,128)(2,1)}, u32[]{:S(2)}) copy-start(bf16[2048,8]{0,1:T(8,128)(2,1)} %param.31) | copy-start | bytes 98308
  6.6 9.0 %copy-start.4 = (bf16[2048,32]{0,1:T(8,128)(2,1)S(1)}, bf16[2048,32]{0,1:T(8,128)(2,1)}, u32[]{:S(2)}) copy-start(bf16[2048,32]{0,1:T(8,128)(2,1)} %param.36) | copy-start | bytes 393220
  6.6 162.7 %all-gather.9.cloned.1.call-start = ((), (), s32[]{:S(2)}) async-start(), calls=%async_computation.1 | async-start | bytes 7987200 | tf_op jit(solution)/shard_map/all_gather | solution.py:23
  10.4 0.6 copy-start.3
  11.1 243.0 %all-gather.11.cloned.1.call-start = ((), (), s32[]{:S(2)}) async-start(), calls=%async_computation.2 | async-start | bytes 1671168 | tf_op jit(solution)/shard_map/all_gather | solution.py:23
  16.6 166.4 %copy-start.11 = (f32[256]{0:T(256)S(1)}, f32[256]{0:T(256)}, u32[]{:S(2)}) copy-start(f32[256]{0:T(256)} %param.38) | copy-start | bytes 3076
  183.9 131.5 %all-gather.15.cloned.1.call-start = ((), (), s32[]{:S(2)}) async-start(), calls=%async_computation.4 | async-start | bytes 4456448 | tf_op jit(solution)/shard_map/all_gather | solution.py:46
  230.2 5.2 %copy-start.7 = (bf16[512,32]{0,1:T(8,128)(2,1)S(1)}, bf16[512,32]{0,1:T(8,128)(2,1)}, u32[]{:S(2)}) copy-start(bf16[512,32]{0,1:T(8,128)(2,1)} %param.42) | copy-start | bytes 98308
  230.2 5.2 %copy-start.8 = (bf16[512,32]{0,1:T(8,128)(2,1)S(1)}, bf16[512,32]{0,1:T(8,128)(2,1)}, u32[]{:S(2)}) copy-start(bf16[512,32]{0,1:T(8,128)(2,1)} %param.41) | copy-start | bytes 98308
  230.8 15.4 %copy-start.12 = (f32[128]{0:T(128)S(1)}, f32[128]{0:T(128)}, u32[]{:S(2)}) copy-start(f32[128]{0:T(128)} %param.33) | copy-start | bytes 1540
  232.6 157.5 %all-gather.17.cloned.1.call-start = ((), (), s32[]{:S(2)}) async-start(), calls=%async_computation.5 | async-start | bytes 4456448 | tf_op jit(solution)/shard_map/all_gather | solution.py:46
  233.5 13.5 %copy-start.10 = (f32[512]{0:T(512)S(1)}, f32[512]{0:T(512)}, u32[]{:S(2)}) copy-start(f32[512]{0:T(512)} %param.37) | copy-start | bytes 6148
  235.3 229.4 %all-gather.13.cloned.1.call-start = ((), (), s32[]{:S(2)}) async-start(), calls=%async_computation.3 | async-start | bytes 4456448 | tf_op jit(solution)/shard_map/all_gather | solution.py:66
  251.1 3.0 copy-start.1
  390.1 1.0 copy-start.2
  482.4 0.7 copy-start.9
Sparse Core Ops, SparseCore 0:
  11.2 157.9 all-gather.8
  184.0 55.3 all-gather.10
  241.3 74.1 all-gather.14
  317.1 72.9 all-gather.16
  391.7 72.9 all-gather.12
where the time goes:
time: 492 us; the launch traced here: 490 us
  waiting for transfers between devices  339 us (69%)
  other arithmetic  52.8 us (11%)
  blocking collectives  34.7 us (7%)
  matrix products  32.6 us (7%)
  local copies, waits for them, and re-layouts  16.3 us (3%)
  between operations  13.9 us (3%)
    all_gather x2, waiting for transfers between devices, sent_together(): filled = lax.all_gather(both, axis, axis=dim, tiled=True)  153 us
    all_gather x2, waiting for transfers between devices, prefix(): lax.all_gather(a.astype(kind), axis)  114 us
    all_gather x1, waiting for transfers between devices, gather_axes(): nearer = lax.all_gather(array, axes[-1], axis=dim, tiled=True)  72.3 us
    another operation x1, other arithmetic, delta_terms(): jax.scipy.linalg.solve_triangular(identity + lower_mat, jnp.broadcast_to(...  39.3 us
    all_to_all x1, blocking collectives, copy_for_each(): lax.all_to_all(jnp.broadcast_to(array[None], (devices, *array.shape)), ax...  13.9 us
    all_gather x1, blocking collectives, gather_axes(): nearer = lax.all_gather(array, axes[-1], axis=dim, tiled=True)  10.6 us
    all_gather x1, blocking collectives, one_gather(): lines, at, done = (lax.all_gather(vector, axis), 0, [])  10.2 us
  transfers between devices with their start and end apart: 5, of which 4 were waited for; matrix products, arithmetic and copies ran while one was open for 18% of the time, Pallas kernels for 0%

commit v1 on v0

v1 whole, which is shorter than its diff:
```python
import functools
import math

import jax
import jax.numpy as jnp
from jax import lax
from jax.experimental import pallas as pl
from jax.experimental.pallas import tpu as pltpu
from jax.sharding import PartitionSpec as P

HEAD = 128
NOPE = 64
ROPE = 32
VDIM = 64
BLOCK = 64
LANES = 128

NORM_EPS = 1e-06
ROPE_THETA = 10000.0
F32 = jnp.float32
BF16 = jnp.bfloat16
MESH = pl.DeviceIdType.MESH
VM = pltpu.VMEM


def remote(src, dst, send_sem, recv_sem, where):
    return pltpu.make_async_remote_copy(
        src_ref=src,
        dst_ref=dst,
        send_sem=send_sem,
        recv_sem=recv_sem,
        device_id=where,
        device_id_type=MESH,
    )


def greet(places, count):
    barrier = pltpu.get_barrier_semaphore()
    for place in places:
        pl.semaphore_signal(barrier, inc=1, device_id=place, device_id_type=MESH)
    pl.semaphore_wait(barrier, count)


def mm(left, right):
    return lax.dot_general(
        left.astype(BF16), right.astype(BF16), (((1,), (0,)), ((), ())), preferred_element_type=F32
    )


def mm_nt(left, right):
    return lax.dot_general(
        left.astype(BF16), right.astype(BF16), (((1,), (1,)), ((), ())), preferred_element_type=F32
    )


def project_kernel(
    nz, nx, tok_ref, wp_ref, out_ref, toks, ws,
    loc_sem, tok_send, tok_recv, fwd_send, fwd_recv, wx_send, wx_recv, r_send, r_recv, l_send, l_recv,
):
    z, x, t = lax.axis_index("sp"), lax.axis_index("fs"), lax.axis_index("tp")
    rows = wp_ref.shape[1]
    right, left = {"sp": lax.rem(z + 1, nz)}, {"sp": lax.rem(z + nz - 1, nz)}
    partner = {"tp": 1 - t}
    others = [lax.rem(x + d, nx) for d in range(1, nx)]
    greet([{"fs": o} for o in others] + [right, left, partner], nx + 2)

    def chunk(slot, part):
        return ws.at[slot, pl.ds(part * rows, rows)]

    own_w = pltpu.make_async_copy(wp_ref.at[x], chunk(z, x), loc_sem.at[0])
    own_w.start()
    wx = [
        remote(wp_ref.at[o], chunk(z, x), wx_send.at[d], wx_recv.at[d], {"fs": o})
        for d, o in enumerate(others)
    ]
    for copy in wx:
        copy.start()
    own_t = pltpu.make_async_copy(tok_ref, toks.at[pl.ds(2 * x, 2)], loc_sem.at[1])
    own_t.start()
    tok = [
        remote(tok_ref.at[t], toks.at[2 * x + t], tok_send.at[d], tok_recv.at[d], {"fs": o})
        for d, o in enumerate(others)
    ]
    for copy in tok:
        copy.start()

    reach_r, reach_l = nz // 2, nz // 2 - 1

    def go_right(step, part, slot):
        return remote(
            chunk(slot, part), chunk(slot, part), r_send.at[step, part], r_recv.at[step, part], right
        )

    def go_left(step, part, slot):
        return remote(
            chunk(slot, part), chunk(slot, part), l_send.at[step, part], l_recv.at[step, part], left
        )

    for d in range(nx):
        part = lax.rem(x + nx - d, nx)
        if d == 0:
            own_w.wait()
        else:
            wx[d - 1].wait_recv()
        go_right(0, part, z).start()
        go_left(0, part, z).start()

    def ring(step, carry):
        from_left = lax.rem(z + 2 * nz - 1 - step, nz)
        from_right = lax.rem(z + 1 + step, nz)
        for d in range(nx):
            part = lax.rem(x + nx - d, nx)
            go_right(step, part, from_left).wait_recv()

            @pl.when(step < reach_r - 1)
            def _():
                go_right(step + 1, part, from_left).start()

            @pl.when(step < reach_l)
            def _():
                go_left(step, part, from_right).wait_recv()

            @pl.when(step < reach_l - 1)
            def _():
                go_left(step + 1, part, from_right).start()

        return carry

    lax.fori_loop(0, reach_r, ring, 0)

    own_t.wait()
    fwd = []
    for d in range(nx - 1):
        source = lax.rem(x + nx - 1 - d, nx)
        tok[d].wait_recv()
        copy = remote(
            toks.at[2 * source + t], toks.at[2 * source + t], fwd_send.at[d], fwd_recv.at[d], partner
        )
        copy.start()
        fwd.append(copy)
    for copy in fwd:
        copy.wait_recv()

    depth = ws.shape[0] * ws.shape[1]
    weight = ws[...].reshape(depth, ws.shape[2])
    pair = 2 * toks.shape[1]

    def tile(i, carry):
        lhs = toks[pl.ds(2 * i, 2)].reshape(pair, depth)
        out_ref[pl.ds(pl.multiple_of(i * pair, pair), pair), :] = lax.dot_general(
            lhs, weight, (((1,), (0,)), ((), ())), preferred_element_type=F32
        )
        return carry

    lax.fori_loop(0, nx, tile, 0)

    for copy in wx + tok + fwd:
        copy.wait_send()

    def drain(step, carry):
        for part in range(nx):
            go_right(step, part, z).wait_send()

            @pl.when(step < reach_l)
            def _():
                go_left(step, part, z).wait_send()

        return carry

    lax.fori_loop(0, reach_r, drain, 0)


def project(nz, nx, normed, packed):
    seqs, length, width = normed.shape
    rows, cols = packed.shape[1:]
    dma = pltpu.SemaphoreType.DMA
    return pl.pallas_call(
        functools.partial(project_kernel, nz, nx),
        out_shape=jax.ShapeDtypeStruct((seqs * nx * length, cols), F32),
        in_specs=[pl.BlockSpec(memory_space=VM)] * 2,
        out_specs=pl.BlockSpec(memory_space=VM),
        scratch_shapes=[
            VM((seqs * nx, length, width), BF16),
            VM((nz, nx * rows, cols), BF16),
            dma((2,)),
            dma((nx - 1,)),
            dma((nx - 1,)),
            dma((nx - 1,)),
            dma((nx - 1,)),
            dma((nx - 1,)),
            dma((nx - 1,)),
            dma((nz // 2, nx)),
            dma((nz // 2, nx)),
            dma((nz // 2 - 1, nx)),
            dma((nz // 2 - 1, nx)),
        ],
        compiler_params=pltpu.CompilerParams(collective_id=1, has_side_effects=True),
        name="project",
    )(normed, packed)


def spread_kernel(
    nz, nx, d_ref, g_ref, l_ref, dr, gr, lr,
    loc_sem, d_send, d_recv, g_send, g_recv, l_send, l_recv,
):
    z, x, t = lax.axis_index("sp"), lax.axis_index("fs"), lax.axis_index("tp")
    half = nz // 2
    zh, zl = z // half, lax.rem(z, half)
    near = [
        (dx, dt, lax.rem(x + dx, nx), lax.rem(t + dt, 2), lax.rem(x + nx - dx, nx))
        for dx in range(nx)
        for dt in range(2)
        if dx or dt
    ]
    sources = [{"fs": back, "tp": to} for dx, dt, fx, to, back in near]
    sources += [{"sp": half * t + j, "tp": 1 - zh} for j in range(half)]
    greet(sources, len(sources))
    own = pltpu.make_async_copy(l_ref.at[x], lr.at[2 * x + t], loc_sem.at[0])
    own.start()
    copies = []
    for k, (dx, dt, fx, to, back) in enumerate(near):
        copies.append(
            remote(l_ref.at[fx], lr.at[2 * x + t], l_send.at[k], l_recv.at[k], {"fs": fx, "tp": to})
        )
    for s in range(half):
        where = {"sp": s + half * (1 - t), "tp": zh}
        copies.append(remote(g_ref.at[s], gr.at[zl], g_send.at[s], g_recv.at[zl], where))
        copies.append(remote(d_ref.at[s], dr.at[zl], d_send.at[s], d_recv.at[zl], where))
    for copy in copies:
        copy.start()
    for k, (dx, dt, fx, to, back) in enumerate(near):
        slot = lr.at[2 * back + to]
        remote(slot, slot, l_send.at[k], l_recv.at[k], {"fs": back, "tp": to}).wait_recv()
    for j in range(half):
        where = {"sp": half * t + j, "tp": 1 - zh}
        remote(gr.at[j], gr.at[j], g_send.at[j], g_recv.at[j], where).wait_recv()
        remote(dr.at[j], dr.at[j], d_send.at[j], d_recv.at[j], where).wait_recv()
    own.wait()
    for copy in copies:
        copy.wait_send()


def spread(nz, nx, blocks, gates, latents):
    half = nz // 2
    dma = pltpu.SemaphoreType.DMA
    near = 2 * nx - 1
    return pl.pallas_call(
        functools.partial(spread_kernel, nz, nx),
        out_shape=(
            jax.ShapeDtypeStruct((half, *blocks.shape[1:]), BF16),
            jax.ShapeDtypeStruct((half, *gates.shape[1:]), F32),
            jax.ShapeDtypeStruct((2 * nx, *latents.shape[1:]), BF16),
        ),
        in_specs=[pl.BlockSpec(memory_space=VM)] * 3,
        out_specs=(pl.BlockSpec(memory_space=VM),) * 3,
        scratch_shapes=[
            dma((1,)),
            dma((half,)),
            dma((half,)),
            dma((half,)),
            dma((half,)),
            dma((near,)),
            dma((near,)),
        ],
        compiler_params=pltpu.CompilerParams(collective_id=2, has_side_effects=True),
        name="spread",
    )(blocks, gates, latents)


def unit(values):
    return values * lax.rsqrt(jnp.sum(values * values, axis=-1, keepdims=True) + NORM_EPS)


def swish(values):
    return values * (1.0 / (1.0 + jnp.exp(-values)))


def delta_kernel(
    nz, nx, raw_ref, gate_ref, gain_ref, out_ref, state_out, state_in, ready,
    st_send, st_recv, h_send, h_recv,
):
    z, x, t = lax.axis_index("sp"), lax.axis_index("fs"), lax.axis_index("tp")
    half = nz // 2
    zh, zl = z // half, lax.rem(z, half)
    lane_t = 1 - zh
    sources = [
        {"fs": xl, "sp": 2 * x + sl + half * (1 - t), "tp": zh} for sl in range(2) for xl in range(nx)
    ]
    greet(sources + [{"tp": 1 - t}], half + 1)

    size = 2 * BLOCK
    row = lax.broadcasted_iota(jnp.int32, (size, size), 0)
    col = lax.broadcasted_iota(jnp.int32, (size, size), 1)
    eye = row == col
    same = (row // BLOCK) == (col // BLOCK)
    strict = same & (row > col)
    causal = same & (row >= col)
    wide_row = lax.broadcasted_iota(jnp.int32, (size, 2 * size), 0)

    def upright(line, where):
        return jnp.sum(jnp.where(where, line, 0.0), axis=1, keepdims=True)

    kept = []
    for p in range(half // 2):
        block = raw_ref[2 * p : 2 * p + 2].reshape(size, 3 * HEAD).astype(F32)
        q = unit(swish(block[:, :HEAD])) * HEAD**-0.5
        k = unit(swish(block[:, HEAD : 2 * HEAD]))
        v = swish(block[:, 2 * HEAD :])
        lines = gate_ref[2 * p] + gate_ref[2 * p + 1]
        beta_row, gate_row = lines[0:1], lines[1:2]
        beta, gate = upright(beta_row, eye), upright(gate_row, eye)
        last = upright(gate_row, col == (row // BLOCK) * BLOCK + BLOCK - 1)
        decay = jnp.exp(jnp.where(causal, gate - gate_row, 0.0))
        lower = jnp.where(strict, beta * mm_nt(k, k) * decay, 0.0)
        scores = jnp.where(causal, mm_nt(q, k) * decay, 0.0)
        inverse = jnp.where(eye, 1.0, 0.0) - jnp.where((row // 2 == col // 2), lower, 0.0)
        width = 2
        while width < BLOCK:
            pick = (row // (2 * width) == col // (2 * width)) & (row // width != col // width)
            inverse = inverse - mm(mm(inverse, jnp.where(pick, lower, 0.0)), inverse)
            width *= 2
        both = mm(inverse, jnp.concatenate([beta * v, beta * k * jnp.exp(gate)], axis=1))
        key_t = (k * jnp.exp(last - gate)).T
        moves = [
            mm(key_t, jnp.where(wide_row // BLOCK == h, both, 0.0)) for h in range(2)
        ]
        factors = [jnp.exp(last[h * BLOCK : h * BLOCK + 1]) for h in range(2)]
        kept.append((q * jnp.exp(gate), scores, both, moves, factors))

    total = jnp.concatenate([jnp.zeros((size, size), F32), jnp.where(eye, 1.0, 0.0)], axis=1)
    states = []
    for j in range(half):
        states.append(total)
        move, factor = kept[j // 2][3][j % 2], kept[j // 2][4][j % 2]
        grown = factor * total - mm(move[:, size:], total)
        total = jnp.concatenate([grown[:, :size] + move[:, :size], grown[:, size:]], axis=1)

    state_out[...] = total[:, :size]
    crossing = remote(state_out, state_in, st_send.at[0], st_recv.at[0], {"tp": 1 - t})

    @pl.when(t == 0)
    def _():
        state_in[...] = jnp.zeros_like(state_in)
        crossing.start()

    @pl.when(t == 1)
    def _():
        crossing.wait_recv()

    start = state_in[...]
    for p in range(half // 2):
        queries, scores, both, _, _ = kept[p]
        read, fixed = [], []
        for h in range(2):
            j = 2 * p + h
            state = states[j][:, :size] + mm(states[j][:, size:], start)
            span = slice(h * BLOCK, (h + 1) * BLOCK)
            got = mm(jnp.concatenate([both[span, size:], queries[span]], axis=0), state)
            fixed.append(both[span, :size] - got[:BLOCK])
            read.append(got[BLOCK:])
        raw = jnp.concatenate(read, axis=0) + mm(scores, jnp.concatenate(fixed, axis=0))
        raw = raw * lax.rsqrt(jnp.mean(raw * raw, axis=-1, keepdims=True) + NORM_EPS)
        heads = (raw * gain_ref[...]).astype(BF16)
        ready[2 * p] = heads[:BLOCK]
        ready[2 * p + 1] = heads[BLOCK:]

    home = [
        remote(
            ready.at[j],
            out_ref.at[lax.rem(zl, 2), x],
            h_send.at[j],
            h_recv.at[lax.rem(zl, 2), x],
            {"fs": zl // 2, "sp": half * t + j, "tp": lane_t},
        )
        for j in range(half)
    ]
    for copy in home:
        copy.start()
    for sl in range(2):
        for xl in range(nx):
            slot = out_ref.at[sl, xl]
            where = {"fs": xl, "sp": 2 * x + sl + half * (1 - t), "tp": zh}
            remote(slot, slot, h_send.at[0], h_recv.at[sl, xl], where).wait_recv()
    for copy in home:
        copy.wait_send()

    @pl.when(t == 0)
    def _():
        crossing.wait_send()


def delta(nz, nx, raw, gates, gain):
    half = nz // 2
    dma = pltpu.SemaphoreType.DMA
    return pl.pallas_call(
        functools.partial(delta_kernel, nz, nx),
        out_shape=jax.ShapeDtypeStruct((2, nx, BLOCK, HEAD), BF16),
        in_specs=[pl.BlockSpec(memory_space=VM)] * 3,
        out_specs=pl.BlockSpec(memory_space=VM),
        scratch_shapes=[
            VM((HEAD, HEAD), F32),
            VM((HEAD, HEAD), F32),
            VM((half, BLOCK, HEAD), BF16),
            dma((1,)),
            dma((1,)),
            dma((half,)),
            dma((2, nx)),
        ],
        compiler_params=pltpu.CompilerParams(collective_id=3, has_side_effects=True),
        name="delta",
    )(raw, gates, gain)


def sent_together(arrays, axis, dim, along):
    widths = [a.shape[along] for a in arrays]
    both = jnp.concatenate(arrays, axis=along)
    filled = lax.all_gather(both, axis, axis=dim, tiled=True)
    return tuple(jnp.split(filled, [sum(widths[:k]) for k in range(1, len(widths))], axis=along))


def gather_axes(array, axes, dim):
    if not axes:
        return array
    nearer = lax.all_gather(array, axes[-1], axis=dim, tiled=True)
    return gather_axes(nearer, axes[:-1], dim)


def copy_for_each(array, axis):
    devices = lax.axis_size(axis)
    return lax.all_to_all(
        jnp.broadcast_to(array[None], (devices, *array.shape)), axis, 0, 0, tiled=True
    )


def taken_together(array, axis):
    return copy_for_each(array, axis).astype(jnp.float32).sum(axis=0)


def stored(values):
    return lax.optimization_barrier(values.astype(jnp.bfloat16))


def rms_scale(values):
    return lax.rsqrt(jnp.mean(values * values, axis=-1, keepdims=True) + NORM_EPS)


def rope_tables(positions, rope_width):
    frequency = ROPE_THETA ** (-jnp.arange(0, rope_width, 2, dtype=jnp.float32) / rope_width)
    angles = positions.astype(jnp.float32)[:, None] * frequency[None, :]
    return (jnp.cos(angles), jnp.sin(angles))


def rotate(values, cosine_table, sine_table):
    lower_half, upper_half = jnp.split(values, 2, axis=-1)
    return jnp.concatenate(
        [
            lower_half * cosine_table - upper_half * sine_table,
            upper_half * cosine_table + lower_half * sine_table,
        ],
        axis=-1,
    )


def keep_same(current):
    return current


def local(
    tokens,
    pre_gain,
    query_weight,
    key_weight,
    value_weight,
    beta_weight,
    decay_weight,
    decay_rate,
    delta_gain,
    query_down,
    latent_down,
    rope_weight,
    query_gain,
    latent_gain,
    query_up,
    latent_up,
    delta_out,
    latent_out,
    post_gain,
):
    f32 = jnp.float32
    seq_count, token_count = (tokens.shape[0], tokens.shape[1])
    row_total = seq_count * token_count
    sequence = tokens.reshape(row_total, tokens.shape[2]).astype(f32)
    query_start = lax.axis_index("sp") * token_count
    positions = query_start + jnp.arange(token_count)
    normed = (sequence * rms_scale(sequence) * pre_gain).astype(jnp.bfloat16)
    head_group = lax.axis_index("tp")
    nz, nx = lax.axis_size("sp"), lax.axis_size("fs")
    z, x = lax.axis_index("sp"), lax.axis_index("fs")
    row_span = query_weight.shape[0]
    row_start = (z * nx + x) * row_span

    def own_rows(array):
        return lax.dynamic_slice_in_dim(array, row_start, row_span, 0)

    def for_cores(array):
        parts = array.reshape(row_span, nx, 2, -1)
        return lax.dynamic_index_in_dim(parts, head_group, 2, False)

    def for_heads(array):
        parts = array.reshape(row_span, 2, nx, -1)
        return lax.dynamic_index_in_dim(parts, head_group, 1, False)

    q_width = query_down.shape[1] // (2 * nx)
    kv_width = latent_down.shape[1] // (2 * nx)
    rope_width = rope_weight.shape[1] // (2 * nx)
    side = jnp.concatenate(
        [
            for_cores(query_down),
            for_cores(latent_down),
            for_cores(own_rows(rope_weight)),
            for_heads(own_rows(beta_weight)),
            for_heads(own_rows(decay_weight)),
        ],
        axis=-1,
    )
    at_beta = q_width + kv_width + rope_width
    side = jnp.pad(side, ((0, 0), (0, 0), (0, LANES - side.shape[-1])))
    packed = jnp.concatenate(
        [w.reshape(row_span, nx, HEAD) for w in (query_weight, key_weight, value_weight)] + [side],
        axis=-1,
    )
    packed = jnp.moveaxis(packed, 1, 0)
    projected = project(nz, nx, normed.reshape(seq_count, token_count, -1), packed)
    lanes = nx * seq_count
    blocks = projected[:, : 3 * HEAD].astype(jnp.bfloat16).reshape(lanes, token_count, 3 * HEAD)
    latents = projected[:, 3 * HEAD :].astype(jnp.bfloat16).reshape(nx, row_total, LANES)
    at_beta += 3 * HEAD
    beta_gate = jax.nn.sigmoid(projected[:, at_beta]).reshape(lanes, token_count)
    own_rate = lax.dynamic_index_in_dim(decay_rate, head_group * nx + x, 0, False)
    log_decay = -own_rate * jax.nn.softplus(projected[:, at_beta + 1]).reshape(lanes, token_count)
    gate_sum = jnp.cumsum(log_decay, axis=-1)
    lines = jnp.stack([beta_gate, gate_sum], axis=1)
    empty = jnp.zeros_like(lines)
    odd = lax.rem(z, 2) == 1
    lines = jnp.concatenate([jnp.where(odd, empty, lines), jnp.where(odd, lines, empty)], axis=-1)
    lines = jnp.pad(lines, ((0, 0), (0, 6), (0, 0)))
    blocks_in, lines_in, latents_in = spread(nz, nx, blocks, lines, latents)
    homed = delta(nz, nx, blocks_in, lines_in, delta_gain.reshape(1, HEAD))
    delta_heads = jnp.transpose(homed, (0, 2, 1, 3)).reshape(row_total, nx * HEAD)

    def joined(start, width):
        return jnp.moveaxis(latents_in[:, :, start : start + width], 0, 1).reshape(row_total, -1)

    q_latent = joined(0, q_width)
    kv_latent = joined(q_width, kv_width)
    rope_raw = joined(q_width + kv_width, rope_width)
    q_lat32 = q_latent.astype(f32)
    kv_lat32 = kv_latent.astype(f32)
    q_normed = (q_lat32 * rms_scale(q_lat32) * query_gain).astype(jnp.bfloat16)
    kv_normed = (kv_lat32 * rms_scale(kv_lat32) * latent_gain).astype(jnp.bfloat16)
    cosine_table, sine_table = rope_tables(positions, rope_raw.shape[1])
    rope_keys = rotate(
        rope_raw.astype(f32).reshape(seq_count, token_count, rope_raw.shape[1]),
        cosine_table,
        sine_table,
    ).astype(jnp.bfloat16)
    latent_count = query_up.shape[1] // (NOPE + ROPE)
    query_all = stored(jnp.dot(q_normed, query_up, preferred_element_type=f32)).reshape(
        seq_count, token_count, latent_count, NOPE + ROPE
    )
    query_plain = query_all[..., :NOPE]
    query_turned = rotate(
        query_all[..., NOPE:].astype(f32), cosine_table[:, None, :], sine_table[:, None, :]
    ).astype(jnp.bfloat16)
    score_scale = (NOPE + ROPE) ** (-0.5)
    query_block = positions // BLOCK
    kv_seq = kv_normed.reshape(seq_count, token_count, kv_normed.shape[1])

    def attend_block(totals, key_plain, value_rows, rope_rows, key_start):
        row_max, row_sum, weighted = totals
        key_block = (key_start + jnp.arange(key_plain.shape[1])) // BLOCK
        allowed = key_block[None, :] <= query_block[:, None]
        logits = (
            jnp.einsum("sqhd,skhd->shqk", query_plain, key_plain, preferred_element_type=f32)
            + jnp.einsum("sqhd,skd->shqk", query_turned, rope_rows, preferred_element_type=f32)
        ) * score_scale
        logits = jnp.where(allowed[None, None], logits, -jnp.inf)
        new_max = jnp.maximum(row_max, jnp.max(logits, axis=-1))
        shift = jnp.where(jnp.isfinite(new_max), new_max, 0.0)
        weights = jnp.where(allowed[None, None], jnp.exp(logits - shift[..., None]), 0.0)
        rescale = jnp.exp(row_max - shift)
        row_sum = row_sum * rescale + jnp.sum(weights, axis=-1)
        weighted = weighted * rescale[..., None] + jnp.einsum(
            "shqk,skhd->shqd", weights.astype(jnp.bfloat16), value_rows, preferred_element_type=f32
        )
        return (new_max, row_sum, weighted)

    start_stats = (
        jnp.full((seq_count, latent_count, token_count), -jnp.inf, f32),
        jnp.zeros((seq_count, latent_count, token_count), f32),
        jnp.zeros((seq_count, latent_count, token_count, VDIM), f32),
    )

    def expand_latent(portion, row_start, span_rows):
        latent_rows = lax.dynamic_slice_in_dim(portion[0], row_start, span_rows, 1)
        expanded = jnp.dot(
            latent_rows.reshape(seq_count * span_rows, latent_rows.shape[2]),
            latent_up,
            preferred_element_type=f32,
        ).astype(jnp.bfloat16)
        expanded = expanded.reshape(seq_count, span_rows, latent_count, NOPE + VDIM)
        return (
            expanded[..., :NOPE],
            expanded[..., NOPE:],
            lax.dynamic_slice_in_dim(portion[1], row_start, span_rows, 1),
        )

    portion = sent_together((kv_seq, rope_keys), "sp", 1, 2)
    row_count = portion[0].shape[1]
    span_rows = math.gcd(row_count, token_count * max(1, 512 // token_count))

    def visit_rows(current):

        def visit_block(block_index, stats):
            row_start = block_index * span_rows
            key_plain, value_rows, rope_rows = expand_latent(portion, row_start, span_rows)
            return attend_block(stats, key_plain, value_rows, rope_rows, row_start)

        return lax.fori_loop(0, row_count // span_rows, visit_block, current)

    row_max, row_sum, weighted = lax.cond(
        jnp.int32(0) < query_start + token_count, visit_rows, keep_same, start_stats
    )
    latent_heads = (
        jnp.transpose(weighted / row_sum[..., None], (0, 2, 1, 3))
        .reshape(row_total, latent_count * VDIM)
        .astype(jnp.bfloat16)
    )
    heads_joined = jnp.concatenate([delta_heads, latent_heads], axis=1)
    out_rows = jnp.concatenate([delta_out, latent_out], axis=0)
    partial_value = jnp.dot(
        heads_joined, gather_axes(out_rows, ("sp", "fs"), 1), preferred_element_type=f32
    )
    whole_rows = taken_together(partial_value.astype(jnp.bfloat16), "tp").astype(jnp.float32)
    row_scale = rms_scale(whole_rows)
    half_width = post_gain.shape[0]
    own_half = lax.dynamic_slice_in_dim(whole_rows, head_group * half_width, half_width, 1)
    result = own_half * row_scale * post_gain
    return result.astype(jnp.bfloat16).reshape(seq_count, token_count, result.shape[1])


def solution(mesh):
    return jax.shard_map(
        local,
        mesh=mesh,
        in_specs=(
            P(("grp", "fs"), "sp", None),
            P(),
            P(("sp", "fs"), "tp"),
            P(("sp", "fs"), "tp"),
            P(("sp", "fs"), "tp"),
            P(),
            P(),
            P(),
            P(),
            P(("sp", "fs"), None),
            P(("sp", "fs"), None),
            P(),
            P(),
            P(),
            P(None, "tp"),
            P(None, "tp"),
            P("tp", ("sp", "fs")),
            P("tp", ("sp", "fs")),
            P("tp"),
        ),
        out_specs=P(("grp", "fs"), "sp", "tp"),
        check_vma=False,
    )
```

time: 492 us -> 287 us (0.58)
  waiting for transfers between devices: 339 us -> 66.4 us
  Pallas kernels: 0 us -> 117 us
  other arithmetic: 52.8 us -> 18.8 us
  matrix products: 32.6 us -> 14.9 us
  local copies, waits for them, and re-layouts: 16.3 us -> 30 us
  blocking collectives: 34.7 us -> 23.8 us
    all_gather x2 -> x1, waiting for transfers between devices: 153 us -> 23.9 us  [sent_together(): filled = lax.all_gather(both, axis, axis=dim, tiled=True)]
    pallas_call x0 -> x3, Pallas kernels: none -> 117 us  [the longest x1 63.9 us: project(): pl.pallas_call(functools.partial(project_kernel, nz, nx), out_shape=jax.S...]
    all_gather x2 -> x0, waiting for transfers between devices: 114 us -> none  [prefix(): lax.all_gather(a.astype(kind), axis)]
    another operation x4, other arithmetic: 39.7 us -> 1.58 us  [the longest x1 39.3 us: delta_terms(): jax.scipy.linalg.solve_triangular(identity + lower_mat, jnp.broadcast_to(...]
    all_gather x1, waiting for transfers between devices: 72.3 us -> 42.5 us  [gather_axes(): nearer = lax.all_gather(array, axes[-1], axis=dim, tiled=True)]
    dot_general x21 -> x0, matrix products: 19.1 us -> none  [the longest x5 8.99 us: local(): jnp.dot(normed, weight, preferred_element_type=f32)]
    all_gather x1 -> x0, blocking collectives: 10.2 us -> none  [one_gather(): lines, at, done = (lax.all_gather(vector, axis), 0, [])]
  transfers between devices with their start and end apart: 5 -> 2, of which waited for: 4 -> 2; matrix products, arithmetic and copies ran while one was open for 18% -> 13% of each run, Pallas kernels for 0% -> 11%
where the time goes in v1:
time: 287 us; the launch traced here: 286 us
  Pallas kernels  117 us (41%)
  waiting for transfers between devices  66.4 us (23%)
  local copies, waits for them, and re-layouts  30 us (10%)
  blocking collectives  23.8 us (8%)
  other arithmetic  18.8 us (7%)
  matrix products  14.9 us (5%)
  between operations  14.5 us (5%)
    pallas_call x1, Pallas kernels, project(): pl.pallas_call(functools.partial(project_kernel, nz, nx), out_shape=jax.S...  63.9 us
    all_gather x1, waiting for transfers between devices, gather_axes(): nearer = lax.all_gather(array, axes[-1], axis=dim, tiled=True)  42.5 us
    pallas_call x1, Pallas kernels, delta(): pl.pallas_call(functools.partial(delta_kernel, nz, nx), out_shape=jax.Sha...  30.8 us
    all_gather x1, waiting for transfers between devices, sent_together(): filled = lax.all_gather(both, axis, axis=dim, tiled=True)  23.9 us
    pallas_call x1, Pallas kernels, spread(): pl.pallas_call(functools.partial(spread_kernel, nz, nx), out_shape=(jax.S...  22.7 us
    all_to_all x1, blocking collectives, copy_for_each(): lax.all_to_all(jnp.broadcast_to(array[None], (devices, *array.shape)), ax...  13.6 us
    all_gather x1, blocking collectives, gather_axes(): nearer = lax.all_gather(array, axes[-1], axis=dim, tiled=True)  10.2 us
    another operation x3, local copies, waits for them, and re-layouts  6.03 us
  transfers between devices with their start and end apart: 2, of which 2 were waited for; matrix products, arithmetic and copies ran while one was open for 13% of the time, Pallas kernels for 11%

profile of v1, /device:TPU:33, one launch (start us, length us, event | category | flops | bytes accessed | tf_op | source)
XLA Modules:
  0.0 286.0 jit_solution(13791430376780211344)
XLA Ops:
  6.6 0.8 constant_dynamic-slice_fusion.4
  7.4 0.8 constant_dynamic-slice_fusion.2
  8.4 0.8 constant_dynamic-slice_fusion.6
  9.3 0.8 reshape.384
  10.2 0.9 reshape.383
  11.2 0.8 copy_bitcast_fusion.3
  12.0 1.2 fusion.23
  13.2 0.8 copy_bitcast_fusion.1
  14.0 2.0 fusion.25.tok_ref
  16.2 0.7 fusion.37.wp_ref
  16.9 63.9 %project.1 = f32[512,512]{1,0:T(8,128)} custom-call(bf16[2,64,2048]{2,1,0:T(8,128)(2,1)} %fusion.25.tok_ref, bf16[4,32,512]{2,1,0:T(8,128)(2,1)} %fusion.37.wp_ref), custom_call_target="tpu_custom_call" | custom-call | tf_op jit(solution)/shard_map/project/pallas_call | solution.py:177
  80.8 1.4 fusion.34
  82.2 1.3 convert.22
  83.5 0.8 slice.68
  86.7 0.7 select_maximum_fusion.1.g_ref
  87.4 22.7 %spread.1 = (bf16[8,64,384]{2,1,0:T(8,128)(2,1)}, f32[8,8,128]{2,1,0:T(8,128)}, bf16[8,128,128]{2,1,0:T(8,128)(2,1)}) custom-call(bf16[8,64,384]{2,1,0:T(8,128)(2,1)} %bitcast.110, f32[8,8,128]{2,1,0:T(8,128)} %select_maximum_fusion.1.g_ref, bf16[4,128,128]{2,1,0:T(8,128)(2,1)} %bitcast.112), custom_call_target="tpu_custom_call" | custom-call | tf_op jit(solution)/shard_map/spread/pallas_call | solution.py:247
  110.1 1.1 convert_bitcast_fusion.2
  111.2 1.2 fusion.26
  112.4 1.2 convert_bitcast_fusion.3
  115.1 0.8 copy.115
  116.1 10.2 %all_gather.10 = bf16[1024,128]{0,1:T(8,128)(2,1)} all-gather(bf16[1024,32]{0,1:T(8,128)(2,1)S(1)} %pad_maximum_fusion.2), channel_id=1, replica_groups=mesh['grp'=2,'sp'=16,'fs'=4,'tp'=2] {'fs'}, dimensions={1}, use_global_device_ids=true | all-gather | bytes 327680 | tf_op jit(solution)/shard_map/all_gather | solution.py:424
  127.9 30.8 %delta.1 = bf16[2,4,64,128]{3,2,1,0:T(8,128)(2,1)} custom-call(bf16[8,64,384]{2,1,0:T(8,128)(2,1)} %get-tuple-element.410.raw_ref, f32[8,8,128]{2,1,0:T(8,128)} %get-tuple-element.411.gate_ref, f32[1,128]{1,0:T(1,128)} %bitcast.123), custom_call_target="tpu_custom_call" | custom-call | tf_op jit(solution)/shard_map/delta/pallas_call | solution.py:395
  158.6 1.0 copy.112
  160.4 0.7 pad_maximum_fusion.1
  161.1 23.9 %all-gather.3.cloned.1.call-done = bf16[2,1024,288]{2,0,1:T(2,128)(2,1)} async-done(((bf16[2,64,288]{2,0,1:T(2,128)(2,1)}), bf16[2,1024,288]{2,0,1:T(2,128)(2,1)}) %all-gather.3.cloned.1.call-update) | async-done | bytes 1179664 | tf_op jit(solution)/shard_map/all_gather | solution.py:417
  184.9 31.1 %conditional.1 = (f32[2,8,64]{2,1,0:T(8,128)}, f32[2,8,64,64]{3,2,1,0:T(8,128)}) conditional(s32[]{:T(128)} %convert_element_type.117, () %tuple.51, (bf16[2,1024,288]{2,0,1:T(2,128)(2,1)}, s32[64]{0:T(128)S(1)}, s32[64]{0:T(128)S(1)}, s32[]{:T(128)}, bf16[2,64,8,96]{3,2,1,0:T(8,128)(2,1)S(1)}, /*index=5*/bf16[256,1024]{1,0:T(8,128)(2,1)S(1)}, ...), branch_computations={%region_4.5_spmd, %region_5.10_spmd.clone} | conditional | flops 711182272 | bytes 43394500 | solution.py:631
  184.9 1.7 copy.99
  186.7 1.2 split.34
  187.8 3.6 %copy.118 = bf16[2,1024,288]{1,2,0:T(8,128)(2,1)} copy(bf16[2,1024,288]{2,0,1:T(2,128)(2,1)S(1)} %copy-done.4) | data formatting | bytes 2359296 | tf_op jit(solution)/shard_map
  191.4 1.6 split.35
  192.9 0.8 copy.119
  193.7 22.3 %while.32 = (s32[]{:T(128)}, f32[2,8,64]{2,1,0:T(8,128)S(1)}, f32[2,8,64]{2,1,0:T(8,128)}, f32[2,8,64,64]{3,2,1,0:T(8,128)}, s32[64]{0:T(128)S(1)}, /*index=5*/b...) while((s32[]{:T(128)}, f32[2,8,64]{2,1,0:T(8,128)S(1)}, ...), condition=%wide.region_9.9_spmd.clone, body=%wide.region_6.8_spmd.clone.sunk | while | flops 711181312 | bytes 31203868 | solution.py:629
  193.7 1.1 constant_dynamic-slice_fusion.10
  194.8 0.7 convert_bitcast_fusion.5
  196.1 2.0 fusion.75
  198.2 1.8 fusion.76
  202.4 1.7 fusion.80
  204.1 1.1 constant_dynamic-slice_fusion.10
  205.2 0.7 convert_bitcast_fusion.5
  206.5 2.0 fusion.75
  208.6 1.8 fusion.76
  211.9 1.3 fusion.79
  213.2 2.8 fusion.80
  216.0 1.3 fusion.33
  217.6 42.5 %all-gather.5.cloned.1.call-done = bf16[1024,2048]{0,1:T(8,128)(2,1)} async-done(((bf16[1024,128]{0,1:T(8,128)(2,1)}), bf16[1024,2048]{0,1:T(8,128)(2,1)}) %all-gather.5.cloned.1.call-update) | async-done | bytes 4194320 | tf_op jit(solution)/shard_map/all_gather | solution.py:424
  260.1 3.8 %convolution_convert_fusion = bf16[128,2048]{1,0:T(8,128)(2,1)S(1)} fusion(bf16[1024,2048]{0,1:T(8,128)(2,1)} %all-gather.5.cloned.1.call-done, bf16[128,512]{1,0:T(8,128)(2,1)S(1)} %convert_element_type.136, bf16[128,512]{1,0:T(8,128)(2,1)} %bitcast.111), kind=kOutput, calls=%fused_computation.40 | convolution fusion | flops 537657344 | bytes 4980736 | tf_op jit(solution)/shard_map/dot_general | solution.py:641
  264.0 13.6 %all_to_all.5 = bf16[2,128,2048]{2,1,0:T(8,128)(2,1)S(1)} all-to-all(bf16[2,128,2048]{2,1,0:T(8,128)(2,1)S(1)} %broadcast_in_dim.125), channel_id=1, replica_groups=mesh['grp'=2,'sp'=16,'fs'=4,'tp'=2] {'tp'}, dimensions={0} | all-to-all | bytes 2097152 | tf_op jit(solution)/shard_map/all_to_all | solution.py:430
  278.3 0.8 multiply_convert_fusion
  (105 shorter events, 12.4 us)
Async XLA Ops:
  6.5 120.3 %copy-start = (bf16[512,768]{1,0:T(8,128)(2,1)S(1)}, bf16[512,768]{1,0:T(8,128)(2,1)}, u32[]{:S(2)}) copy-start(bf16[512,768]{1,0:T(8,128)(2,1)} %param.37) | copy-start | bytes 2359300
  6.6 178.4 %all-gather.3.cloned.1.call-start = ((), (), s32[]{:S(2)}) async-start(), calls=%async_computation.1 | async-start | bytes 1671168 | tf_op jit(solution)/shard_map/all_gather | solution.py:417
  16.8 68.2 %copy-start.12 = (f32[8]{0:T(128)S(1)}, f32[8]{0:T(128)}, u32[]{:S(2)}) copy-start(f32[8]{0:T(128)} %param.30) | copy-start | bytes 100
  85.0 29.5 %copy-start.11 = (f32[256]{0:T(256)S(1)}, f32[256]{0:T(256)}, u32[]{:S(2)}) copy-start(f32[256]{0:T(256)} %param.36) | copy-start | bytes 3076
  111.2 4.8 %copy-start.7 = (bf16[512,32]{0,1:T(8,128)(2,1)S(1)}, bf16[512,32]{0,1:T(8,128)(2,1)}, u32[]{:S(2)}) copy-start(bf16[512,32]{0,1:T(8,128)(2,1)} %param.40) | copy-start | bytes 98308
  111.2 4.8 %copy-start.8 = (bf16[512,32]{0,1:T(8,128)(2,1)S(1)}, bf16[512,32]{0,1:T(8,128)(2,1)}, u32[]{:S(2)}) copy-start(bf16[512,32]{0,1:T(8,128)(2,1)} %param.39) | copy-start | bytes 98308
  112.4 13.9 %copy-start.3 = (bf16[8,128,128]{2,1,0:T(8,128)(2,1)S(1)}, bf16[8,128,128]{2,1,0:T(8,128)(2,1)}, u32[]{:S(2)}) copy-start(bf16[8,128,128]{2,1,0:T(8,128)(2,1)} %get-tuple-element.412) | copy-start | bytes 786436
  114.1 12.7 %copy-start.10 = (f32[512]{0:T(512)S(1)}, f32[512]{0:T(512)}, u32[]{:S(2)}) copy-start(f32[512]{0:T(512)} %param.35) | copy-start | bytes 6148
  116.0 144.1 %all-gather.5.cloned.1.call-start = ((), (), s32[]{:S(2)}) async-start(), calls=%async_computation.2 | async-start | bytes 4456448 | tf_op jit(solution)/shard_map/all_gather | solution.py:424
  126.9 58.0 %copy-start.2 = (bf16[256,1024]{1,0:T(8,128)(2,1)S(1)}, bf16[256,1024]{1,0:T(8,128)(2,1)}, u32[]{:S(2)}) copy-start(bf16[256,1024]{1,0:T(8,128)(2,1)} %param.38) | copy-start | bytes 1572868
  184.9 2.9 %copy-start.4 = (bf16[2,1024,288]{2,0,1:T(2,128)(2,1)S(1)}, bf16[2,1024,288]{2,0,1:T(2,128)(2,1)}, u32[]{:S(2)}) copy-start(bf16[2,1024,288]{2,0,1:T(2,128)(2,1)} %get-tuple-element.497) | copy-start | bytes 3538948 | tf_op jit(solution)/shard_map/cond
  198.2 2.0 copy-start.5
  198.2 2.0 copy-start.6
  200.8 1.6 copy-start.1
  208.6 2.0 copy-start.5
  208.6 2.0 copy-start.6
  211.2 2.0 copy-start.1
  277.6 0.7 copy-start.9
Sparse Core Ops, SparseCore 0:
  116.1 68.7 all-gather.2
  186.7 73.3 all-gather.4

commit v2 on v1

v2 whole, which is shorter than its diff:
```python
import functools
import math

import jax
import jax.numpy as jnp
from jax import lax
from jax.experimental import pallas as pl
from jax.experimental.pallas import tpu as pltpu
from jax.sharding import PartitionSpec as P

HEAD = 128
NOPE = 64
ROPE = 32
VDIM = 64
BLOCK = 64
LANES = 128

NORM_EPS = 1e-06
ROPE_THETA = 10000.0
F32 = jnp.float32
BF16 = jnp.bfloat16
MESH = pl.DeviceIdType.MESH
VM = pltpu.VMEM


def remote(src, dst, send_sem, recv_sem, where):
    return pltpu.make_async_remote_copy(
        src_ref=src,
        dst_ref=dst,
        send_sem=send_sem,
        recv_sem=recv_sem,
        device_id=where,
        device_id_type=MESH,
    )


def greet(places, count):
    barrier = pltpu.get_barrier_semaphore()
    for place in places:
        pl.semaphore_signal(barrier, inc=1, device_id=place, device_id_type=MESH)
    pl.semaphore_wait(barrier, count)


def mm(left, right):
    return lax.dot_general(
        left.astype(BF16), right.astype(BF16), (((1,), (0,)), ((), ())), preferred_element_type=F32
    )


def mm_nt(left, right):
    return lax.dot_general(
        left.astype(BF16), right.astype(BF16), (((1,), (1,)), ((), ())), preferred_element_type=F32
    )


def project_kernel(
    nz, nx, tok_ref, wp_ref, wt_ref, out_ref, wz_ref, toks, ws,
    loc_sem, tok_send, tok_recv, fwd_send, fwd_recv, wx_send, wx_recv, r_send, r_recv, l_send, l_recv,
):
    z, x, t = lax.axis_index("sp"), lax.axis_index("fs"), lax.axis_index("tp")
    rows = wp_ref.shape[1]
    right, left = {"sp": lax.rem(z + 1, nz)}, {"sp": lax.rem(z + nz - 1, nz)}
    partner = {"tp": 1 - t}
    others = [lax.rem(x + d, nx) for d in range(1, nx)]
    greet([{"fs": o} for o in others] + [right, left, partner], nx + 2)

    def chunk(slot, part):
        if part is None:
            return wz_ref.at[slot]
        return ws.at[slot, pl.ds(part * rows, rows)]

    def mark(part):
        return nx if part is None else part

    own_w = pltpu.make_async_copy(wp_ref.at[x], chunk(z, x), loc_sem.at[0])
    own_w.start()
    wx = [
        remote(wp_ref.at[o], chunk(z, x), wx_send.at[d], wx_recv.at[d], {"fs": o})
        for d, o in enumerate(others)
    ]
    for copy in wx:
        copy.start()
    own_o = pltpu.make_async_copy(wt_ref, wz_ref.at[z], loc_sem.at[2])
    own_o.start()
    own_t = pltpu.make_async_copy(tok_ref, toks.at[pl.ds(2 * x, 2)], loc_sem.at[1])
    own_t.start()
    tok = [
        remote(tok_ref.at[t], toks.at[2 * x + t], tok_send.at[d], tok_recv.at[d], {"fs": o})
        for d, o in enumerate(others)
    ]
    for copy in tok:
        copy.start()

    reach_r, reach_l = nz // 2, nz // 2 - 1

    def go_right(step, part, slot):
        return remote(
            chunk(slot, part), chunk(slot, part), r_send.at[step, mark(part)], r_recv.at[step, mark(part)], right
        )

    def go_left(step, part, slot):
        return remote(
            chunk(slot, part), chunk(slot, part), l_send.at[step, mark(part)], l_recv.at[step, mark(part)], left
        )

    for d in range(nx):
        part = lax.rem(x + nx - d, nx)
        if d == 0:
            own_w.wait()
        else:
            wx[d - 1].wait_recv()
        go_right(0, part, z).start()
        go_left(0, part, z).start()
    own_o.wait()
    go_right(0, None, z).start()
    go_left(0, None, z).start()

    def ring(step, carry):
        from_left = lax.rem(z + 2 * nz - 1 - step, nz)
        from_right = lax.rem(z + 1 + step, nz)
        for d in range(nx + 1):
            part = lax.rem(x + nx - d, nx) if d < nx else None
            go_right(step, part, from_left).wait_recv()

            @pl.when(step < reach_r - 1)
            def _():
                go_right(step + 1, part, from_left).start()

            @pl.when(step < reach_l)
            def _():
                go_left(step, part, from_right).wait_recv()

            @pl.when(step < reach_l - 1)
            def _():
                go_left(step + 1, part, from_right).start()

        return carry

    lax.fori_loop(0, reach_r, ring, 0)

    own_t.wait()
    fwd = []
    for d in range(nx - 1):
        source = lax.rem(x + nx - 1 - d, nx)
        tok[d].wait_recv()
        copy = remote(
            toks.at[2 * source + t], toks.at[2 * source + t], fwd_send.at[d], fwd_recv.at[d], partner
        )
        copy.start()
        fwd.append(copy)
    for copy in fwd:
        copy.wait_recv()

    depth = ws.shape[0] * ws.shape[1]
    weight = ws[...].reshape(depth, ws.shape[2])
    pair = 2 * toks.shape[1]

    def tile(i, carry):
        lhs = toks[pl.ds(2 * i, 2)].reshape(pair, depth)
        out_ref[pl.ds(pl.multiple_of(i * pair, pair), pair), :] = lax.dot_general(
            lhs, weight, (((1,), (0,)), ((), ())), preferred_element_type=F32
        )
        return carry

    lax.fori_loop(0, nx, tile, 0)

    for copy in wx + tok + fwd:
        copy.wait_send()

    def drain(step, carry):
        for part in [*range(nx), None]:
            go_right(step, part, z).wait_send()

            @pl.when(step < reach_l)
            def _():
                go_left(step, part, z).wait_send()

        return carry

    lax.fori_loop(0, reach_r, drain, 0)


def project(nz, nx, normed, packed, out_cols):
    seqs, length, width = normed.shape
    rows, cols = packed.shape[1:]
    dma = pltpu.SemaphoreType.DMA
    return pl.pallas_call(
        functools.partial(project_kernel, nz, nx),
        out_shape=(
            jax.ShapeDtypeStruct((seqs * nx * length, cols), F32),
            jax.ShapeDtypeStruct((nz, *out_cols.shape), BF16),
        ),
        in_specs=[pl.BlockSpec(memory_space=VM)] * 3,
        out_specs=(pl.BlockSpec(memory_space=VM),) * 2,
        scratch_shapes=[
            VM((seqs * nx, length, width), BF16),
            VM((nz, nx * rows, cols), BF16),
            dma((3,)),
            dma((nx - 1,)),
            dma((nx - 1,)),
            dma((nx - 1,)),
            dma((nx - 1,)),
            dma((nx - 1,)),
            dma((nx - 1,)),
            dma((nz // 2, nx + 1)),
            dma((nz // 2, nx + 1)),
            dma((nz // 2 - 1, nx + 1)),
            dma((nz // 2 - 1, nx + 1)),
        ],
        compiler_params=pltpu.CompilerParams(collective_id=1, has_side_effects=True),
        name="project",
    )(normed, packed, out_cols)


def unit(values):
    return values * lax.rsqrt(jnp.sum(values * values, axis=-1, keepdims=True) + NORM_EPS)


def swish(values):
    return values * (1.0 / (1.0 + jnp.exp(-values)))


def mix_kernel(
    nz, nx, d_ref, g_ref, l_ref, wz_ref, qup_ref, qgain_ref, kvgain_ref, wuk_ref, wuv_ref,
    cos_ref, sin_ref, dgain_ref, pgain_ref, out_ref,
    dr, gr, lr, kvg, wo, homed, ready, state_out, state_in, part_out, part_in,
    loc_sem, a_send, a_recv, d_send, d_recv, g_send, g_recv, kr_send, kr_recv, kl_send, kl_recv,
    kp_send, kp_recv, w_send, w_recv, st_send, st_recv, h_send, h_recv, p_send, p_recv,
):
    z, x, t = lax.axis_index("sp"), lax.axis_index("fs"), lax.axis_index("tp")
    half = nz // 2
    zh, zl = z // half, lax.rem(z, half)
    lane_t = 1 - zh
    partner = {"tp": 1 - t}
    near = [
        (dx, dt, lax.rem(x + dx, nx), lax.rem(t + dt, 2), lax.rem(x + nx - dx, nx))
        for dx in range(nx)
        for dt in range(2)
        if dx or dt
    ]
    right, left = {"sp": lax.rem(z + 1, nz)}, {"sp": lax.rem(z + nz - 1, nz)}
    east, west = {"fs": lax.rem(x + 1, nx)}, {"fs": lax.rem(x + nx - 1, nx)}
    sources = [{"fs": back, "tp": to} for dx, dt, fx, to, back in near]
    sources += [right, left]
    sources += [{"sp": half * t + j, "tp": 1 - zh} for j in range(half)]
    sources += [
        {"fs": xl, "sp": 2 * x + sl + half * (1 - t), "tp": zh} for sl in range(2) for xl in range(nx)
    ]
    greet(sources, len(sources))
    started = []

    def begin(copy):
        copy.start()
        started.append(copy)
        return copy

    own_l = pltpu.make_async_copy(l_ref.at[x], lr.at[2 * x + t], loc_sem.at[0])
    own_l.start()
    for k, (dx, dt, fx, to, back) in enumerate(near):
        begin(
            remote(l_ref.at[fx], lr.at[2 * x + t], a_send.at[k], a_recv.at[k], {"fs": fx, "tp": to})
        )

    def send_lane(s):
        where = {"sp": s + half * (1 - t), "tp": zh}
        begin(remote(g_ref.at[s], gr.at[zl], g_send.at[s], g_recv.at[zl], where))
        begin(remote(d_ref.at[s], dr.at[zl], d_send.at[s], d_recv.at[zl], where))

    send_lane(0)
    send_lane(1)

    def w_part(owner, upper):
        return wo.at[pl.ds(half * upper, half), owner]

    own_w = pltpu.make_async_copy(wz_ref, wo.at[:, x], loc_sem.at[1])
    own_w.start()
    for upper, where, k in ((0, east, 0), (1, west, 1), (1, east, 2), (0, west, 3)):
        begin(
            remote(
                wz_ref.at[pl.ds(half * upper, half)], w_part(x, upper), w_send.at[k], w_recv.at[k], where
            )
        )

    for k, (dx, dt, fx, to, back) in enumerate(near):
        slot = lr.at[2 * back + to]
        remote(slot, slot, a_send.at[k], a_recv.at[k], {"fs": back, "tp": to}).wait_recv()
    own_l.wait()

    cores = 2 * nx
    rows = lr.shape[1]
    count = rows // BLOCK
    lane = lax.broadcasted_iota(jnp.int32, (rows, LANES), 1)
    q_width, kv_width = qup_ref.shape[0] // cores // 2, wuv_ref.shape[1] // cores
    at_rope = q_width + kv_width
    rope_width = ROPE // cores
    parts = [lr[c].astype(F32) for c in range(cores)]
    q_square = sum(jnp.where(lane < q_width, part * part, 0.0) for part in parts)
    kv_square = sum(
        jnp.where((lane >= q_width) & (lane < at_rope), part * part, 0.0) for part in parts
    )
    q_scale = lax.rsqrt(jnp.sum(q_square, axis=-1, keepdims=True) / (q_width * cores) + NORM_EPS)
    kv_scale = lax.rsqrt(jnp.sum(kv_square, axis=-1, keepdims=True) / (kv_width * cores) + NORM_EPS)
    from_lane = lax.broadcasted_iota(jnp.int32, (LANES, 4 * LANES), 0)
    to_lane = lax.broadcasted_iota(jnp.int32, (LANES, 4 * LANES), 1)
    kv_total = kv_width * cores
    slab = jnp.zeros((rows, 4 * LANES), F32)
    for c in range(cores):
        kept = jnp.where(lane < at_rope, parts[c] * kv_scale * kvgain_ref[c], parts[c])
        is_kv = (from_lane >= q_width) & (from_lane < at_rope)
        is_rope = (from_lane >= at_rope) & (from_lane < at_rope + rope_width)
        entry = from_lane - at_rope + rope_width * c
        spot = to_lane - kv_total
        place = jnp.where(
            is_kv & (to_lane == from_lane - q_width + kv_width * c), 1.0, 0.0
        )
        spot_in = spot % ROPE
        straight = is_rope & (spot >= 0) & (spot < LANES) & (spot_in == entry)
        swapped = is_rope & (spot >= LANES) & ((spot_in + ROPE // 2) % ROPE == entry)
        sign = jnp.where(spot_in < ROPE // 2, -1.0, 1.0)
        place = place + jnp.where(straight, 1.0, 0.0) + jnp.where(swapped, sign, 0.0)
        slab = slab + mm(kept, place)
    turned = slab[:, kv_total : kv_total + LANES].astype(BF16).astype(F32) * cos_ref[...]
    turned = turned + slab[:, kv_total + LANES :].astype(BF16).astype(F32) * sin_ref[...]
    keys = jnp.concatenate([slab[:, :kv_total], turned], axis=1).astype(BF16)
    for s in range(count):
        kvg[s, z] = keys[s * BLOCK : (s + 1) * BLOCK]

    def go_right(step, slot):
        return remote(kvg.at[t, slot], kvg.at[t, slot], kr_send.at[step], kr_recv.at[step], right)

    def go_left(step, slot):
        return remote(kvg.at[t, slot], kvg.at[t, slot], kl_send.at[step], kl_recv.at[step], left)

    def across(slot, k):
        return remote(kvg.at[t, slot], kvg.at[t, slot], kp_send.at[k], kp_recv.at[k], partner)

    begin(go_right(0, z))
    begin(go_left(0, z))

    q_rows = jnp.concatenate(
        [(parts[c] * q_scale * qgain_ref[c]).astype(BF16) for c in range(cores)], axis=1
    )
    query = mm(q_rows, qup_ref[...]).astype(BF16)
    heads = wuv_ref.shape[0]
    plain_width = heads * NOPE
    turn_width = heads * ROPE
    stacked = [[] for _ in range(count)]
    for h in range(heads):
        base = (h // 2) * LANES
        mine = (lane // NOPE) == h % 2
        plain = jnp.where(mine, query[:, base : base + LANES].astype(F32), 0.0)
        absorbed = mm(plain, wuk_ref[h // 2]).astype(BF16)
        base = plain_width + (h * ROPE // LANES) * LANES
        raw = query[:, base : base + LANES].astype(F32)
        swap = query[:, base + turn_width : base + turn_width + LANES].astype(F32)
        turn = raw * cos_ref[...] + swap * sin_ref[...]
        turn = jnp.where((lane // ROPE) == h % (LANES // ROPE), turn, 0.0).astype(BF16)
        joined = jnp.concatenate([absorbed, turn], axis=1)
        for s in range(count):
            stacked[s].append(joined[s * BLOCK : (s + 1) * BLOCK])

    reach_r, reach_l = nz // 2, nz // 2 - 1
    for step in range(reach_r):
        if step + 2 < half:
            send_lane(step + 2)
        from_left = lax.rem(z + 2 * nz - 1 - step, nz)
        from_right = lax.rem(z + 1 + step, nz)
        go_right(step, from_left).wait_recv()
        if step < reach_r - 1:
            begin(go_right(step + 1, from_left))
        begin(across(from_left, step))
        if step < reach_l:
            go_left(step, from_right).wait_recv()
            if step < reach_l - 1:
                begin(go_left(step + 1, from_right))
            begin(across(from_right, reach_r + step))

    remote(w_part(x, 0), w_part(x, 0), w_send.at[0], w_recv.at[0], west).wait_recv()
    begin(
        remote(w_part(lax.rem(x + nx - 1, nx), 0), w_part(lax.rem(x + nx - 1, nx), 0),
               w_send.at[4], w_recv.at[4], east)
    )
    remote(w_part(x, 1), w_part(x, 1), w_send.at[1], w_recv.at[1], east).wait_recv()
    begin(
        remote(w_part(lax.rem(x + 1, nx), 1), w_part(lax.rem(x + 1, nx), 1),
               w_send.at[5], w_recv.at[5], west)
    )

    for j in range(half):
        where = {"sp": half * t + j, "tp": 1 - zh}
        remote(gr.at[j], gr.at[j], g_send.at[j], g_recv.at[j], where).wait_recv()
        remote(dr.at[j], dr.at[j], d_send.at[j], d_recv.at[j], where).wait_recv()

    size = 2 * BLOCK
    row = lax.broadcasted_iota(jnp.int32, (size, size), 0)
    col = lax.broadcasted_iota(jnp.int32, (size, size), 1)
    eye = row == col
    same = (row // BLOCK) == (col // BLOCK)
    strict = same & (row > col)
    causal = same & (row >= col)
    wide_row = lax.broadcasted_iota(jnp.int32, (size, 2 * size), 0)

    def upright(line, where):
        return jnp.sum(jnp.where(where, line, 0.0), axis=1, keepdims=True)

    terms = []
    for p in range(half // 2):
        block = dr[2 * p : 2 * p + 2].reshape(size, 3 * HEAD).astype(F32)
        q = unit(swish(block[:, :HEAD])) * HEAD**-0.5
        k = unit(swish(block[:, HEAD : 2 * HEAD]))
        v = swish(block[:, 2 * HEAD :])
        lines = gr[2 * p] + gr[2 * p + 1]
        beta_row, gate_row = lines[0:1], lines[1:2]
        beta, gate = upright(beta_row, eye), upright(gate_row, eye)
        last = upright(gate_row, col == (row // BLOCK) * BLOCK + BLOCK - 1)
        decay = jnp.exp(jnp.where(causal, gate - gate_row, 0.0))
        lower = jnp.where(strict, beta * mm_nt(k, k) * decay, 0.0)
        scores = jnp.where(causal, mm_nt(q, k) * decay, 0.0)
        inverse = jnp.where(eye, 1.0, 0.0) - jnp.where((row // 2 == col // 2), lower, 0.0)
        width = 2
        while width < BLOCK:
            pick = (row // (2 * width) == col // (2 * width)) & (row // width != col // width)
            inverse = inverse - mm(mm(inverse, jnp.where(pick, lower, 0.0)), inverse)
            width *= 2
        both = mm(inverse, jnp.concatenate([beta * v, beta * k * jnp.exp(gate)], axis=1))
        key_t = (k * jnp.exp(last - gate)).T
        moves = [
            mm(key_t, jnp.where(wide_row // BLOCK == h, both, 0.0)) for h in range(2)
        ]
        factors = [jnp.exp(last[h * BLOCK : h * BLOCK + 1]) for h in range(2)]
        terms.append((q * jnp.exp(gate), scores, both, moves, factors))

    total = jnp.concatenate([jnp.zeros((size, size), F32), jnp.where(eye, 1.0, 0.0)], axis=1)
    states = []
    for j in range(half):
        states.append(total)
        move, factor = terms[j // 2][3][j % 2], terms[j // 2][4][j % 2]
        grown = factor * total - mm(move[:, size:], total)
        total = jnp.concatenate([grown[:, :size] + move[:, :size], grown[:, size:]], axis=1)

    state_out[...] = total[:, :size]
    crossing = remote(state_out, state_in, st_send.at[0], st_recv.at[0], partner)

    @pl.when(t == 0)
    def _():
        state_in[...] = jnp.zeros_like(state_in)
        crossing.start()

    @pl.when(t == 1)
    def _():
        crossing.wait_recv()

    start = state_in[...]
    for p in range(half // 2):
        queries, scores, both, _, _ = terms[p]
        read, fixed = [], []
        for h in range(2):
            j = 2 * p + h
            state = states[j][:, :size] + mm(states[j][:, size:], start)
            span = slice(h * BLOCK, (h + 1) * BLOCK)
            got = mm(jnp.concatenate([both[span, size:], queries[span]], axis=0), state)
            fixed.append(both[span, :size] - got[:BLOCK])
            read.append(got[BLOCK:])
        raw = jnp.concatenate(read, axis=0) + mm(scores, jnp.concatenate(fixed, axis=0))
        raw = raw * lax.rsqrt(jnp.mean(raw * raw, axis=-1, keepdims=True) + NORM_EPS)
        done = (raw * dgain_ref[...]).astype(BF16)
        ready[2 * p] = done[:BLOCK]
        ready[2 * p + 1] = done[BLOCK:]

    for j in range(half):
        begin(
            remote(
                ready.at[j],
                homed.at[lax.rem(zl, 2), x],
                h_send.at[j],
                h_recv.at[lax.rem(zl, 2), x],
                {"fs": zl // 2, "sp": half * t + j, "tp": lane_t},
            )
        )

    for k in range(nz - 1):
        slot = kvg.at[1 - t, lax.rem(z + 1, nz)]
        remote(slot, slot, kp_send.at[k], kp_recv.at[k], partner).wait_recv()
    allowed = lax.broadcasted_iota(jnp.int32, (1, nz * BLOCK), 1) < (z + 1) * BLOCK
    outs = []
    for s in range(count):
        keys = kvg[s].reshape(nz * BLOCK, kvg.shape[3])
        scores = mm_nt(jnp.concatenate(stacked[s], axis=0), keys) * (NOPE + ROPE) ** (-0.5)
        scores = jnp.where(allowed, scores, -1e30)
        peak = jnp.max(scores, axis=-1, keepdims=True)
        weights = jnp.where(allowed, jnp.exp(scores - peak), 0.0)
        total = jnp.sum(weights, axis=-1, keepdims=True)
        mixed = (mm(weights, keys[:, :kv_total]) / total).astype(BF16)
        pairs = []
        for p in range(heads // 2):
            upper = mm(mixed[2 * p * BLOCK : (2 * p + 1) * BLOCK], wuv_ref[2 * p])
            lower_head = mm(mixed[(2 * p + 1) * BLOCK : (2 * p + 2) * BLOCK], wuv_ref[2 * p + 1])
            pairs.append((upper + lower_head).astype(BF16))
        outs.append(jnp.concatenate(pairs, axis=1))
    latent_heads = jnp.concatenate(outs, axis=0)

    own_w.wait()
    for k, owner, upper in (
        (2, lax.rem(x + nx - 1, nx), 1),
        (3, lax.rem(x + 1, nx), 0),
        (4, lax.rem(x + 2, nx), 0),
        (5, lax.rem(x + 2, nx), 1),
    ):
        remote(
            w_part(owner, upper), w_part(owner, upper), w_send.at[k], w_recv.at[k], east
        ).wait_recv()
    for sl in range(2):
        for xl in range(nx):
            slot = homed.at[sl, xl]
            where = {"fs": xl, "sp": 2 * x + sl + half * (1 - t), "tp": zh}
            remote(slot, slot, h_send.at[0], h_recv.at[sl, xl], where).wait_recv()
    delta_heads = [homed[:, xl].reshape(rows, HEAD) for xl in range(nx)]
    joined = jnp.concatenate(delta_heads + [latent_heads], axis=1)
    width = wo.shape[0] * wo.shape[1] * wo.shape[2]
    columns = wo[...].reshape(width, wo.shape[3])
    part_out[...] = mm_nt(joined, columns).astype(BF16)
    swap_parts = begin(remote(part_out, part_in, p_send.at[0], p_recv.at[0], partner))
    swap_parts.wait_recv()
    whole = part_out[...].astype(F32) + part_in[...].astype(F32)
    scale = lax.rsqrt(jnp.mean(whole * whole, axis=-1, keepdims=True) + NORM_EPS)
    own_half = jnp.where(t == 0, whole[:, : width // 2], whole[:, width // 2 :])
    out_ref[...] = (own_half * scale * pgain_ref[...]).astype(BF16)

    for copy in started:
        copy.wait_send()

    @pl.when(t == 0)
    def _():
        crossing.wait_send()


def mix(nz, nx, *operands):
    blocks, gates, latents, out_cols = operands[:4]
    half = nz // 2
    heads = operands[8].shape[0]
    rows = latents.shape[1]
    slab = operands[8].shape[1] + LANES
    width = nz * nx * out_cols.shape[1]
    dma = pltpu.SemaphoreType.DMA
    one = lambda count: [dma((count,)), dma((count,))]
    return pl.pallas_call(
        functools.partial(mix_kernel, nz, nx),
        out_shape=jax.ShapeDtypeStruct((rows, width // 2), BF16),
        in_specs=[pl.BlockSpec(memory_space=VM)] * len(operands),
        out_specs=pl.BlockSpec(memory_space=VM),
        scratch_shapes=[
            VM((half, *blocks.shape[1:]), BF16),
            VM((half, *gates.shape[1:]), F32),
            VM((2 * nx, *latents.shape[1:]), BF16),
            VM((rows // BLOCK, nz, BLOCK, slab), BF16),
            VM((nz, nx, *out_cols.shape[1:]), BF16),
            VM((2, nx, BLOCK, HEAD), BF16),
            VM((half, BLOCK, HEAD), BF16),
            VM((HEAD, HEAD), F32),
            VM((HEAD, HEAD), F32),
            VM((rows, width), BF16),
            VM((rows, width), BF16),
            dma((2,)),
            *one(2 * nx - 1),
            *one(half),
            *one(half),
            *one(nz // 2),
            *one(nz // 2 - 1),
            *one(nz - 1),
            *one(6),
            *one(1),
            dma((half,)),
            dma((2, nx)),
            *one(1),
        ],
        compiler_params=pltpu.CompilerParams(collective_id=2, has_side_effects=True),
        name="mix",
    )(*operands)


def rms_scale(values):
    return lax.rsqrt(jnp.mean(values * values, axis=-1, keepdims=True) + NORM_EPS)


def rope_tables(positions, rope_width):
    frequency = ROPE_THETA ** (-jnp.arange(0, rope_width, 2, dtype=jnp.float32) / rope_width)
    angles = positions.astype(jnp.float32)[:, None] * frequency[None, :]
    return (jnp.cos(angles), jnp.sin(angles))


def local(
    tokens,
    pre_gain,
    query_weight,
    key_weight,
    value_weight,
    beta_weight,
    decay_weight,
    decay_rate,
    delta_gain,
    query_down,
    latent_down,
    rope_weight,
    query_gain,
    latent_gain,
    query_up,
    latent_up,
    delta_out,
    latent_out,
    post_gain,
):
    f32 = jnp.float32
    seq_count, token_count = (tokens.shape[0], tokens.shape[1])
    row_total = seq_count * token_count
    sequence = tokens.reshape(row_total, tokens.shape[2]).astype(f32)
    query_start = lax.axis_index("sp") * token_count
    positions = query_start + jnp.arange(token_count)
    normed = (sequence * rms_scale(sequence) * pre_gain).astype(jnp.bfloat16)
    head_group = lax.axis_index("tp")
    nz, nx = lax.axis_size("sp"), lax.axis_size("fs")
    z, x = lax.axis_index("sp"), lax.axis_index("fs")
    row_span = query_weight.shape[0]
    row_start = (z * nx + x) * row_span

    def own_rows(array):
        return lax.dynamic_slice_in_dim(array, row_start, row_span, 0)

    def for_cores(array):
        parts = array.reshape(row_span, nx, 2, -1)
        return lax.dynamic_index_in_dim(parts, head_group, 2, False)

    def for_heads(array):
        parts = array.reshape(row_span, 2, nx, -1)
        return lax.dynamic_index_in_dim(parts, head_group, 1, False)

    q_width = query_down.shape[1] // (2 * nx)
    kv_width = latent_down.shape[1] // (2 * nx)
    rope_width = rope_weight.shape[1] // (2 * nx)
    side = jnp.concatenate(
        [
            for_cores(query_down),
            for_cores(latent_down),
            for_cores(own_rows(rope_weight)),
            for_heads(own_rows(beta_weight)),
            for_heads(own_rows(decay_weight)),
        ],
        axis=-1,
    )
    at_beta = q_width + kv_width + rope_width
    side = jnp.pad(side, ((0, 0), (0, 0), (0, LANES - side.shape[-1])))
    packed = jnp.concatenate(
        [w.reshape(row_span, nx, HEAD) for w in (query_weight, key_weight, value_weight)] + [side],
        axis=-1,
    )
    packed = jnp.moveaxis(packed, 1, 0)
    out_cols = jnp.concatenate([delta_out, latent_out], axis=0).T
    projected, out_slabs = project(
        nz, nx, normed.reshape(seq_count, token_count, -1), packed, out_cols
    )
    lanes = nx * seq_count
    blocks = projected[:, : 3 * HEAD].astype(jnp.bfloat16).reshape(lanes, token_count, 3 * HEAD)
    latents = projected[:, 3 * HEAD :].astype(jnp.bfloat16).reshape(nx, row_total, LANES)
    at_beta += 3 * HEAD
    beta_gate = jax.nn.sigmoid(projected[:, at_beta]).reshape(lanes, token_count)
    own_rate = lax.dynamic_index_in_dim(decay_rate, head_group * nx + x, 0, False)
    log_decay = -own_rate * jax.nn.softplus(projected[:, at_beta + 1]).reshape(lanes, token_count)
    gate_sum = jnp.cumsum(log_decay, axis=-1)
    lines = jnp.stack([beta_gate, gate_sum], axis=1)
    empty = jnp.zeros_like(lines)
    odd = lax.rem(z, 2) == 1
    lines = jnp.concatenate([jnp.where(odd, empty, lines), jnp.where(odd, lines, empty)], axis=-1)
    lines = jnp.pad(lines, ((0, 0), (0, 6), (0, 0)))
    cores = 2 * nx

    def at_lanes(array, start):
        stop = LANES - start - array.shape[1]
        return jnp.pad(array, ((0, 0), (start, stop)) + ((0, 0),) * (array.ndim - 2))

    q_gain = at_lanes(query_gain.reshape(cores, q_width), 0)[:, None, :]
    kv_gain = at_lanes(latent_gain.reshape(cores, kv_width), q_width)[:, None, :]
    up = query_up.reshape(query_up.shape[0], -1, NOPE + ROPE)
    heads = up.shape[1]
    turn = up[..., NOPE:]
    swap = jnp.concatenate([-turn[..., ROPE // 2 :], turn[..., : ROPE // 2]], axis=-1)
    up = jnp.concatenate(
        [u.reshape(u.shape[0], -1) for u in (up[..., :NOPE], turn, swap)], axis=1
    )
    up = at_lanes(up.reshape(cores, q_width, -1), 0).reshape(cores * LANES, -1)
    pairs = latent_up.reshape(latent_up.shape[0], heads, NOPE + VDIM)
    key_up = jnp.transpose(pairs[..., :NOPE], (1, 2, 0)).reshape(heads // 2, 2 * NOPE, -1)
    value_up = jnp.transpose(pairs[..., NOPE:], (1, 0, 2)).reshape(heads // 2, 2, -1, VDIM)
    value_up = jnp.stack(
        [
            jnp.pad(value_up[:, 0], ((0, 0), (0, 0), (0, VDIM))),
            jnp.pad(value_up[:, 1], ((0, 0), (0, 0), (VDIM, 0))),
        ],
        axis=1,
    ).reshape(heads, -1, 2 * VDIM)
    positions = z * token_count + jnp.arange(token_count)
    tables = rope_tables(positions, ROPE)
    cosine, sine = (jnp.tile(table, (seq_count, LANES // (ROPE // 2))) for table in tables)
    result = mix(
        nz, nx, blocks, lines, latents, out_slabs, up, q_gain, kv_gain, key_up, value_up,
        cosine, sine, delta_gain.reshape(1, HEAD), post_gain.reshape(1, -1),
    )
    return result.reshape(seq_count, token_count, result.shape[1])


def solution(mesh):
    return jax.shard_map(
        local,
        mesh=mesh,
        in_specs=(
            P(("grp", "fs"), "sp", None),
            P(),
            P(("sp", "fs"), "tp"),
            P(("sp", "fs"), "tp"),
            P(("sp", "fs"), "tp"),
            P(),
            P(),
            P(),
            P(),
            P(("sp", "fs"), None),
            P(("sp", "fs"), None),
            P(),
            P(),
            P(),
            P(None, "tp"),
            P(None, "tp"),
            P("tp", ("sp", "fs")),
            P("tp", ("sp", "fs")),
            P("tp"),
        ),
        out_specs=P(("grp", "fs"), "sp", "tp"),
        check_vma=False,
    )
```

time: 287 us -> 176 us (0.61)
  waiting for transfers between devices: 66.4 us -> 0 us
  Pallas kernels: 117 us -> 147 us
  blocking collectives: 23.8 us -> 0 us
  matrix products: 14.9 us -> 0 us
  between operations: 14.5 us -> 0.92 us
  local copies, waits for them, and re-layouts: 30 us -> 17.5 us
  other arithmetic: 18.8 us -> 9.7 us
    all_gather x2 -> x0, waiting for transfers between devices: 66.3 us -> none  [the longest x1 42.5 us: gather_axes(): nearer = lax.all_gather(array, axes[-1], axis=dim, tiled=True)]
    pallas_call x3 -> x2, Pallas kernels: 117 us -> 147 us  [the longest x1 75.3 us: mix(): pl.pallas_call(functools.partial(mix_kernel, nz, nx), out_shape=jax.Shape...]
    dot_general x10 -> x0, matrix products: 14.9 us -> none  [the longest x2 4.49 us: attend_block(): jnp.einsum('shqk,skhd->shqd', weights.astype(jnp.bfloat16), value_rows, p...]
    all_to_all x1 -> x0, blocking collectives: 13.6 us -> none  [copy_for_each(): lax.all_to_all(jnp.broadcast_to(array[None], (devices, *array.shape)), ax...]
    all_gather x1 -> x0, blocking collectives: 10.2 us -> none  [gather_axes(): nearer = lax.all_gather(array, axes[-1], axis=dim, tiled=True)]
    convert_element_type x8 -> x0, other arithmetic: 4.84 us -> none  [the longest x1 1.26 us: local(): latent_heads = jnp.transpose(weighted / row_sum[..., None], (0, 2, 1, 3))...]
    slice x3, local copies, waits for them, and re-layouts: 4.23 us -> 0.8 us  [the longest x1 0.74 us: local(): pairs[..., NOPE:]]
    another operation x3 -> x8, local copies, waits for them, and re-layouts: 6.03 us -> 2.79 us  [the longest x6 1.77 us: local(): jnp.tile(table, (seq_count, LANES // (ROPE // 2)))]
  transfers between devices with their start and end apart: 2 -> 0, of which waited for: 2 -> 0; matrix products, arithmetic and copies ran while one was open for 13% -> 0% of each run, Pallas kernels for 11% -> 0%
where the time goes in v2:
time: 176 us; the launch traced here: 175 us
  Pallas kernels  147 us (84%)
  local copies, waits for them, and re-layouts  17.5 us (10%)
  other arithmetic  9.7 us (6%)
    pallas_call x1, Pallas kernels, mix(): pl.pallas_call(functools.partial(mix_kernel, nz, nx), out_shape=jax.Shape...  75.3 us
    pallas_call x1, Pallas kernels, project(): pl.pallas_call(functools.partial(project_kernel, nz, nx), out_shape=(jax....  71.7 us

profile of v2, /device:TPU:33, one launch (start us, length us, event | category | flops | bytes accessed | tf_op | source)
XLA Modules:
  0.0 175.1 jit_solution(18420166421512719571)
XLA Ops:
  0.0 0.8 constant_dynamic-slice_fusion.3
  0.9 0.8 constant_dynamic-slice_fusion.1
  1.6 0.1 copy.49
  1.7 0.1 copy.50
  1.9 0.1 constant_dynamic-slice_fusion.5
  2.0 0.1 copy.48
  2.1 0.8 reshape.230
  2.9 0.1 constant_dynamic-slice_fusion.6
  3.0 0.9 reshape.229
  3.9 0.1 constant_dynamic-slice_fusion.7
  4.0 0.1 concatenate.25
  4.1 0.8 copy_bitcast_fusion
  4.9 0.8 copy_bitcast_fusion.2
  5.7 0.7 fusion.11.wp_ref
  6.4 1.2 fusion.5
  7.6 1.7 fusion.7.tok_ref
  9.3 0.6 maximum_bitcast_fusion.wt_ref
  9.9 71.7 %project.1 = (f32[512,512]{1,0:T(8,128)}, bf16[16,32,1024]{2,1,0:T(8,128)(2,1)}) custom-call(bf16[2,64,2048]{2,1,0:T(8,128)(2,1)} %fusion.7.tok_ref, bf16[4,32,512]{2,1,0:T(8,128)(2,1)} %fusion.11.wp_ref, bf16[32,1024]{1,0:T(8,128)(2,1)} %maximum_bitcast_fusion.wt_ref), custom_call_target="tpu_custom_call" | custom-call | tf_op jit(solution)/shard_map/project/pallas_call | solution.py:187
  81.7 1.4 fusion.8
  83.1 0.1 squeeze.36
  83.2 0.6 dynamic_slice.40
  84.4 0.2 reduce_window_sum.11
  84.8 0.7 select_maximum_fusion.g_ref
  85.4 1.3 convert.4
  86.7 0.8 slice.52
  87.5 0.7 slice.53
  88.2 0.3 copy.58
  88.5 0.3 concatenate.32
  88.8 0.3 copy.61
  89.2 0.5 reshape.247
  89.7 0.7 copy.67
  90.5 0.3 concatenate.30
  90.8 0.3 copy.60
  91.1 1.6 fusion.4
  92.7 0.2 copy.62
  92.9 0.7 fusion.15
  93.8 1.0 copy.64
  94.8 0.1 multiply_sine_fusion
  95.0 0.1 tile.9
  95.1 0.7 copy.65.cos_ref
  95.9 0.1 tile.21
  96.0 0.7 copy.66.sin_ref
  96.7 0.1 reshape.238
  96.8 0.6 pad.31
  97.4 0.1 reshape.239
  97.5 0.7 pad.32
  98.1 75.3 %mix.1 = bf16[128,1024]{1,0:T(8,128)(2,1)} custom-call(bf16[8,64,384]{2,1,0:T(8,128)(2,1)} %bitcast.79, f32[8,8,128]{2,1,0:T(8,128)} %select_maximum_fusion.g_ref, bf16[4,128,128]{2,1,0:T(8,128)(2,1)} %bitcast.83, bf16[16,32,1024]{2,1,0:T(8,128)(2,1)} %get-tuple-element.8.wz_ref, bf16[1024,1024]{1,0:T(8,128)(2,1)} %bitcast.73, f32[8,1,128]{2,1,0:T(1,128)} %bitcast.90, ...), custom_call_target="tpu_custom_call" | custom-call | tf_op jit(solution)/shard_map/mix/pallas_call | solution.py:546
  173.4 1.7 copy.82
  (37 shorter events, 0.5 us)
Async XLA Ops:
  0.0 1.9 %copy-start = (bf16[2048,32]{0,1:T(8,128)(2,1)S(1)}, bf16[2048,32]{0,1:T(8,128)(2,1)}, u32[]{:S(2)}) copy-start(bf16[2048,32]{0,1:T(8,128)(2,1)} %param.30) | copy-start | bytes 393220
  0.0 7.6 %copy-start.1 = (bf16[2,64,2048]{2,1,0:T(8,128)(2,1)S(1)}, bf16[2,64,2048]{2,1,0:T(8,128)(2,1)}, u32[]{:S(2)}) copy-start(bf16[2,64,2048]{2,1,0:T(8,128)(2,1)} %param.19) | copy-start | bytes 1572868
  0.0 9.3 %copy-start.5 = (bf16[512,32]{0,1:T(8,128)(2,1)S(1)}, bf16[512,32]{0,1:T(8,128)(2,1)}, u32[]{:S(2)}) copy-start(bf16[512,32]{0,1:T(8,128)(2,1)} %param.35) | copy-start | bytes 98308
  0.0 9.3 %copy-start.4 = (bf16[512,32]{0,1:T(8,128)(2,1)S(1)}, bf16[512,32]{0,1:T(8,128)(2,1)}, u32[]{:S(2)}) copy-start(bf16[512,32]{0,1:T(8,128)(2,1)} %param.36) | copy-start | bytes 98308
  2.9 80.3 %copy-start.8 = (f32[8]{0:T(128)S(1)}, f32[8]{0:T(128)}, u32[]{:S(2)}) copy-start(f32[8]{0:T(128)} %param.26) | copy-start | bytes 100
  9.3 78.9 %copy-start.2 = (bf16[512,768]{1,0:T(8,128)(2,1)S(1)}, bf16[512,768]{1,0:T(8,128)(2,1)}, u32[]{:S(2)}) copy-start(bf16[512,768]{1,0:T(8,128)(2,1)} %param.33) | copy-start | bytes 2359300
  90.8 2.0 %copy-start.3 = (bf16[256,1024]{1,0:T(8,128)(2,1)S(1)}, bf16[256,1024]{1,0:T(8,128)(2,1)}, u32[]{:S(2)}) copy-start(bf16[256,1024]{1,0:T(8,128)(2,1)} %param.34) | copy-start | bytes 1572868
  93.7 3.0 %copy-start.6 = (f32[512]{0:T(512)S(1)}, f32[512]{0:T(512)}, u32[]{:S(2)}) copy-start(f32[512]{0:T(512)} %param.31) | copy-start | bytes 6148
  93.7 3.7 %copy-start.7 = (f32[256]{0:T(256)S(1)}, f32[256]{0:T(256)}, u32[]{:S(2)}) copy-start(f32[256]{0:T(256)} %param.32) | copy-start | bytes 3076

commit v3 on v2

v3 whole, which is shorter than its diff:
```python
import functools

import jax
import jax.numpy as jnp
import numpy as np
from jax import lax
from jax.experimental import pallas as pl
from jax.experimental.pallas import tpu as pltpu
from jax.sharding import PartitionSpec as P

HEAD = 128
NOPE = 64
ROPE = 32
VDIM = 64
BLOCK = 64
LANES = 128

NORM_EPS = 1e-06
ROPE_THETA = 10000.0
F32 = jnp.float32
BF16 = jnp.bfloat16
MESH = pl.DeviceIdType.MESH
VM = pltpu.VMEM


def remote(src, dst, send_sem, recv_sem, where):
    return pltpu.make_async_remote_copy(
        src_ref=src,
        dst_ref=dst,
        send_sem=send_sem,
        recv_sem=recv_sem,
        device_id=where,
        device_id_type=MESH,
    )


def greet(places, count):
    barrier = pltpu.get_barrier_semaphore()
    for place in places:
        pl.semaphore_signal(barrier, inc=1, device_id=place, device_id_type=MESH)
    pl.semaphore_wait(barrier, count)


def mm(left, right):
    return lax.dot_general(
        left.astype(BF16), right.astype(BF16), (((1,), (0,)), ((), ())), preferred_element_type=F32
    )


def mm_nt(left, right):
    return lax.dot_general(
        left.astype(BF16), right.astype(BF16), (((1,), (1,)), ((), ())), preferred_element_type=F32
    )


def unit(values):
    return values * lax.rsqrt(jnp.sum(values * values, axis=-1, keepdims=True) + NORM_EPS)


def swish(values):
    return values * (1.0 / (1.0 + jnp.exp(-values)))


def layer_kernel(
    nz, nx, tok_ref, pre_ref, wq_ref, wk_ref, wv_ref, qd_ref, kvd_ref, small_ref, rate_ref, wt_ref,
    qgain_ref, kvgain_ref, qup_ref, lup_ref, far_ref, near_ref, dgain_ref, post_ref, out_ref,
    toks, normed, ws, wz, side, proj, place, blocks, lines_out, latents,
    dr, gr, lr, kvg, wo, homed, ready, state_out, state_in, part_out, part_in,
    loc_sem, wx_send, wx_recv, tok_send, tok_recv, fwd_send, fwd_recv, r_send, r_recv, l_send, l_recv,
    a_send, a_recv, d_send, d_recv, g_send, g_recv, kr_send, kr_recv, kl_send, kl_recv,
    kp_send, kp_recv, w_send, w_recv, st_send, st_recv, h_send, h_recv, p_send, p_recv,
):
    z, x, t = lax.axis_index("sp"), lax.axis_index("fs"), lax.axis_index("tp")
    half = nz // 2
    zh, zl = z // half, lax.rem(z, half)
    lane_t = 1 - zh
    cores = 2 * nx
    span = wq_ref.shape[0]
    rows = tok_ref.shape[0] * tok_ref.shape[1]
    count = rows // BLOCK
    partner = {"tp": 1 - t}
    near = [
        (dx, dt, lax.rem(x + dx, nx), lax.rem(t + dt, 2), lax.rem(x + nx - dx, nx))
        for dx in range(nx)
        for dt in range(2)
        if dx or dt
    ]
    others = [lax.rem(x + d, nx) for d in range(1, nx)]
    right, left = {"sp": lax.rem(z + 1, nz)}, {"sp": lax.rem(z + nz - 1, nz)}
    east, west = {"fs": lax.rem(x + 1, nx)}, {"fs": lax.rem(x + nx - 1, nx)}
    sources = [{"fs": back, "tp": to} for dx, dt, fx, to, back in near]
    sources += [right, left]
    sources += [{"sp": half * t + j, "tp": 1 - zh} for j in range(half)]
    sources += [
        {"fs": xl, "sp": 2 * x + sl + half * (1 - t), "tp": zh} for sl in range(2) for xl in range(nx)
    ]
    greet(sources, len(sources))
    started = []

    def begin(copy):
        copy.start()
        started.append(copy)
        return copy

    def local(src, dst, k):
        copy = pltpu.make_async_copy(src, dst, loc_sem.at[k])
        copy.start()
        return copy

    def chunk(slot, part):
        if part is None:
            return wz.at[slot]
        return ws.at[slot, pl.ds(pl.multiple_of(part * span, span), span)]

    def piece(k):
        return ws.at[z, pl.ds(pl.multiple_of(x * span, span), span), pl.ds(k * LANES, LANES)]

    def columns_of(ref, owner):
        return ref.at[:, pl.ds(pl.multiple_of(owner * LANES, LANES), LANES)]

    mains = (wq_ref, wk_ref, wv_ref)
    for d, o in enumerate(others):
        for k, ref in enumerate(mains):
            begin(
                remote(columns_of(ref, o), piece(k), wx_send.at[d, k], wx_recv.at[d, k], {"fs": o})
            )
    own_w = [local(columns_of(ref, x), piece(k), k) for k, ref in enumerate(mains)]
    own_o = local(wt_ref, wz.at[z], 3)
    own_t = local(tok_ref, toks.at[pl.ds(2 * x, 2)], 4)

    q_width, kv_width = qd_ref.shape[1] // cores, kvd_ref.shape[1] // cores
    rope_width = ROPE // cores
    at_rope = q_width + kv_width
    at_beta = at_rope + rope_width

    def picked(source, lane, first, stop, start):
        return (lane >= first) & (lane < stop) & (source == start + lane - first)

    def ones(mask):
        return jnp.where(mask, 1.0, 0.0)

    def iotas(depth):
        shape = (depth, LANES)
        return lax.broadcasted_iota(jnp.int32, shape, 0), lax.broadcasted_iota(jnp.int32, shape, 1)

    for o in range(nx):
        core, head = 2 * o + t, nx * t + o
        source, lane = iotas(qd_ref.shape[1])
        made = mm(qd_ref[...], ones(picked(source, lane, 0, q_width, q_width * core)))
        source, lane = iotas(kvd_ref.shape[1])
        made += mm(kvd_ref[...], ones(picked(source, lane, q_width, at_rope, kv_width * core)))
        source, lane = iotas(LANES)
        select = picked(source, lane, at_rope, at_beta, rope_width * core)
        select = select | picked(source, lane, at_beta, at_beta + 1, ROPE + head)
        select = select | picked(source, lane, at_beta + 1, at_beta + 2, ROPE + cores + head)
        made += mm(small_ref[...], ones(select))
        side[o] = made.astype(BF16)
    for d, o in enumerate(others):
        k = len(mains)
        begin(remote(side.at[o], piece(k), wx_send.at[d, k], wx_recv.at[d, k], {"fs": o}))
    own_w.append(local(side.at[x], piece(len(mains)), 5))
    for d, o in enumerate(others):
        begin(remote(tok_ref.at[t], toks.at[2 * x + t], tok_send.at[d], tok_recv.at[d], {"fs": o}))

    reach_r, reach_l = nz // 2, nz // 2 - 1

    def go_right(step, part, slot):
        mark = nx if part is None else part
        return remote(
            chunk(slot, part), chunk(slot, part), r_send.at[step, mark], r_recv.at[step, mark], right
        )

    def go_left(step, part, slot):
        mark = nx if part is None else part
        return remote(
            chunk(slot, part), chunk(slot, part), l_send.at[step, mark], l_recv.at[step, mark], left
        )

    for d in range(nx):
        part = lax.rem(x + nx - d, nx)
        if d == 0:
            for copy in own_w:
                copy.wait()
        else:
            for k in range(len(mains) + 1):
                remote(
                    piece(k), piece(k), wx_send.at[d - 1, k], wx_recv.at[d - 1, k], {"fs": part}
                ).wait_recv()
        go_right(0, part, z).start()
        go_left(0, part, z).start()
    own_o.wait()
    go_right(0, None, z).start()
    go_left(0, None, z).start()

    from_lane = lax.broadcasted_iota(jnp.int32, (LANES, 4 * LANES), 0)
    to_lane = lax.broadcasted_iota(jnp.int32, (LANES, 4 * LANES), 1)
    kv_total = kv_width * cores
    spot = to_lane - kv_total
    spot_in = lax.rem(to_lane, ROPE)
    sign = jnp.where(spot_in < ROPE // 2, -1.0, 1.0)
    is_kv = (from_lane >= q_width) & (from_lane < at_rope)
    is_rope = (from_lane >= at_rope) & (from_lane < at_beta)
    for c in range(cores):
        entry = from_lane - at_rope + rope_width * c
        kept = is_kv & (to_lane == from_lane - q_width + kv_width * c)
        straight = is_rope & (spot >= 0) & (spot < LANES) & (spot_in == entry)
        swapped = is_rope & (spot >= LANES) & (lax.rem(spot_in + ROPE // 2, ROPE) == entry)
        place[c] = (ones(kept | straight) + jnp.where(swapped, sign, 0.0)).astype(BF16)

    def ring(step, carry):
        from_left = lax.rem(z + 2 * nz - 1 - step, nz)
        from_right = lax.rem(z + 1 + step, nz)
        for d in range(nx + 1):
            part = lax.rem(x + nx - d, nx) if d < nx else None
            go_right(step, part, from_left).wait_recv()

            @pl.when(step < reach_r - 1)
            def _():
                go_right(step + 1, part, from_left).start()

            @pl.when(step < reach_l)
            def _():
                go_left(step, part, from_right).wait_recv()

            @pl.when(step < reach_l - 1)
            def _():
                go_left(step + 1, part, from_right).start()

        return carry

    early = (reach_r * 5) // 8
    lax.fori_loop(0, early, ring, 0)
    own_t.wait()
    for d in range(nx - 1):
        held = toks.at[2 * lax.rem(x + nx - 1 - d, nx) + t]
        remote(held, held, tok_send.at[d], tok_recv.at[d], partner).wait_recv()
        begin(remote(held, held, fwd_send.at[d], fwd_recv.at[d], partner))
    lax.fori_loop(early, early + 1, ring, 0)
    for d in range(nx - 1):
        held = toks.at[2 * lax.rem(x + nx - 1 - d, nx) + 1 - t]
        remote(held, held, fwd_send.at[d], fwd_recv.at[d], partner).wait_recv()

    def normalize(i, carry):
        values = toks[i].astype(F32)
        scale = lax.rsqrt(jnp.mean(values * values, axis=-1, keepdims=True) + NORM_EPS)
        normed[pl.ds(pl.multiple_of(i * BLOCK, BLOCK), BLOCK), :] = (
            values * scale * pre_ref[...]
        ).astype(BF16)
        return carry

    lax.fori_loop(0, toks.shape[0], normalize, 0)
    lax.fori_loop(early + 1, reach_r - 1, ring, 0)
    depth = ws.shape[1]

    def product(slot):
        lhs = normed[:, pl.ds(pl.multiple_of(slot * depth, depth), depth)]
        return lax.dot_general(lhs, ws[slot], (((1,), (0,)), ((), ())), preferred_element_type=F32)

    def gather_product(i, carry):
        proj[...] += product(lax.rem(z + nz - reach_l + i, nz))
        return carry

    proj[...] = product(z + 0)
    lax.fori_loop(0, reach_l, gather_product, 0)
    lax.fori_loop(reach_l + 1, 2 * reach_l + 1, gather_product, 0)
    lax.fori_loop(reach_r - 1, reach_r, ring, 0)
    proj[...] += product(lax.rem(z + reach_r, nz))

    for o in range(nx):
        latents[o] = proj[o * rows : (o + 1) * rows, 3 * HEAD :].astype(BF16)
    own_l = local(latents.at[x], lr.at[2 * x + t], 0)
    for k, (dx, dt, fx, to, back) in enumerate(near):
        begin(
            remote(latents.at[fx], lr.at[2 * x + t], a_send.at[k], a_recv.at[k], {"fs": fx, "tp": to})
        )

    def w_part(owner, upper):
        return wo.at[pl.ds(half * upper, half), owner]

    own_c = local(wz, wo.at[:, x], 1)
    for upper, where, k in ((0, east, 0), (1, west, 1), (1, east, 2), (0, west, 3)):
        begin(
            remote(wz.at[pl.ds(half * upper, half)], w_part(x, upper), w_send.at[k], w_recv.at[k], where)
        )

    size = 2 * BLOCK
    row = lax.broadcasted_iota(jnp.int32, (size, size), 0)
    col = lax.broadcasted_iota(jnp.int32, (size, size), 1)
    eye = row == col
    same = (row // BLOCK) == (col // BLOCK)
    rate = rate_ref[nx * t + x]
    even = lax.rem(z, 2) == 0
    line = lax.broadcasted_iota(jnp.int32, (8, LANES), 0)
    first_half = lax.broadcasted_iota(jnp.int32, (8, LANES), 1) < LANES // 2
    for p in range(half // 2):
        blocks[2 * p : 2 * p + 2] = (
            proj[p * size : (p + 1) * size, : 3 * HEAD].astype(BF16).reshape(2, BLOCK, 3 * HEAD)
        )
        tail = proj[p * size : (p + 1) * size, 3 * HEAD :]
        write = 1.0 / (1.0 + jnp.exp(-tail[:, at_beta : at_beta + 1]))
        pushed = tail[:, at_beta + 1 : at_beta + 2]
        fade = -rate * (jnp.maximum(pushed, 0.0) + jnp.log1p(jnp.exp(-jnp.abs(pushed))))
        write_row = jnp.sum(jnp.where(eye, write, 0.0), axis=0, keepdims=True)
        fade_row = jnp.sum(jnp.where(same & (row <= col), fade, 0.0), axis=0, keepdims=True)
        both_rows = jnp.where(line == 0, write_row, jnp.where(line == 1, fade_row, 0.0))
        rolled = pltpu.roll(both_rows, LANES // 2, 1)
        lines_out[2 * p] = jnp.where(
            even, jnp.where(first_half, both_rows, 0.0), jnp.where(first_half, 0.0, rolled)
        )
        lines_out[2 * p + 1] = jnp.where(
            even, jnp.where(first_half, rolled, 0.0), jnp.where(first_half, 0.0, both_rows)
        )

    def send_lane(i):
        s = lax.rem(zl + i, half)
        where = {"sp": s + half * (1 - t), "tp": zh}
        begin(remote(lines_out.at[s], gr.at[zl], g_send.at[i], g_recv.at[zl], where))
        begin(remote(blocks.at[s], dr.at[zl], d_send.at[i], d_recv.at[zl], where))

    send_lane(0)
    send_lane(1)

    for k, (dx, dt, fx, to, back) in enumerate(near):
        slot = lr.at[2 * back + to]
        remote(slot, slot, a_send.at[k], a_recv.at[k], {"fs": back, "tp": to}).wait_recv()
    own_l.wait()

    lane = lax.broadcasted_iota(jnp.int32, (rows, LANES), 1)
    far_cos, far_sin = far_ref[0, pl.ds(z, 1), :], far_ref[1, pl.ds(z, 1), :]
    near_cos = jnp.concatenate([near_ref[0]] * count, axis=0)
    near_sin = jnp.concatenate([near_ref[1]] * count, axis=0)
    cosine = far_cos * near_cos - far_sin * near_sin
    sine = far_sin * near_cos + far_cos * near_sin
    slab = mm(lr[0], place[0])
    for c in range(1, cores):
        slab = slab + mm(lr[c], place[c])
    kv_lat = slab[:, :kv_total]
    kv_lat = kv_lat * lax.rsqrt(jnp.mean(kv_lat * kv_lat, axis=-1, keepdims=True) + NORM_EPS)
    turned = slab[:, kv_total : kv_total + LANES] * cosine + slab[:, kv_total + LANES :] * sine
    keys = jnp.concatenate([kv_lat * kvgain_ref[...], turned], axis=1).astype(BF16)
    for s in range(count):
        kvg[s, z] = keys[s * BLOCK : (s + 1) * BLOCK]

    def key_right(step, slot):
        return remote(kvg.at[t, slot], kvg.at[t, slot], kr_send.at[step], kr_recv.at[step], right)

    def key_left(step, slot):
        return remote(kvg.at[t, slot], kvg.at[t, slot], kl_send.at[step], kl_recv.at[step], left)

    def across(slot, k):
        return remote(kvg.at[t, slot], kvg.at[t, slot], kp_send.at[k], kp_recv.at[k], partner)

    begin(key_right(0, z))
    begin(key_left(0, z))

    q_lat = jnp.concatenate(
        [
            jnp.where(
                lane < LANES // 2,
                lr[c].astype(F32),
                pltpu.roll(lr[c + 1].astype(F32), LANES // 2, 1),
            )
            for c in range(0, cores, 2)
        ],
        axis=1,
    )
    q_lat = q_lat * lax.rsqrt(jnp.mean(q_lat * q_lat, axis=-1, keepdims=True) + NORM_EPS)
    query = mm(q_lat * qgain_ref[...], qup_ref[...]).astype(BF16).astype(F32)
    head_width = NOPE + ROPE
    heads = query.shape[1] // head_width
    is_turn = (lane >= NOPE) & (lane < head_width)
    from_turn = (row >= NOPE) & (row < head_width)
    low_turn = (col >= NOPE) & (col < NOPE + ROPE // 2)
    high_turn = (col >= NOPE + ROPE // 2) & (col < head_width)
    exchange = jnp.where(from_turn & high_turn & (row == col - ROPE // 2), 1.0, 0.0)
    exchange = exchange - jnp.where(from_turn & low_turn & (row == col + ROPE // 2), 1.0, 0.0)
    stacked = [[] for _ in range(count)]
    for h in range(heads):
        own = query[:, h * head_width : (h + 1) * head_width]
        own = jnp.concatenate([own, jnp.zeros((rows, LANES - head_width), F32)], axis=1)
        absorbed = mm_nt(
            jnp.where(lane < NOPE, own, 0.0), lup_ref[:, h * LANES : (h + 1) * LANES]
        )
        turn = jnp.where(is_turn, own * cosine + mm(own, exchange) * sine, 0.0)
        joined = jnp.concatenate([absorbed, turn], axis=1).astype(BF16)
        for s in range(count):
            stacked[s].append(joined[s * BLOCK : (s + 1) * BLOCK])

    for step in range(reach_r):
        if step + 2 < half:
            send_lane(step + 2)
        from_left = lax.rem(z + 2 * nz - 1 - step, nz)
        from_right = lax.rem(z + 1 + step, nz)
        key_right(step, from_left).wait_recv()
        if step < reach_r - 1:
            begin(key_right(step + 1, from_left))
        begin(across(from_left, step))
        if step < reach_l:
            key_left(step, from_right).wait_recv()
            if step < reach_l - 1:
                begin(key_left(step + 1, from_right))
            begin(across(from_right, reach_r + step))

    behind, ahead = lax.rem(x + nx - 1, nx), lax.rem(x + 1, nx)
    remote(w_part(behind, 0), w_part(behind, 0), w_send.at[0], w_recv.at[0], west).wait_recv()
    begin(remote(w_part(behind, 0), w_part(behind, 0), w_send.at[4], w_recv.at[4], east))
    remote(w_part(ahead, 1), w_part(ahead, 1), w_send.at[1], w_recv.at[1], east).wait_recv()
    begin(remote(w_part(ahead, 1), w_part(ahead, 1), w_send.at[5], w_recv.at[5], west))

    for j in range(half):
        where = {"sp": half * t + j, "tp": 1 - zh}
        remote(gr.at[j], gr.at[j], g_send.at[j], g_recv.at[j], where).wait_recv()
        remote(dr.at[j], dr.at[j], d_send.at[j], d_recv.at[j], where).wait_recv()

    strict = same & (row > col)
    causal = same & (row >= col)
    wide_row = lax.broadcasted_iota(jnp.int32, (size, 2 * size), 0)

    def upright(line, where):
        return jnp.sum(jnp.where(where, line, 0.0), axis=1, keepdims=True)

    terms = []
    for p in range(half // 2):
        block = dr[2 * p : 2 * p + 2].reshape(size, 3 * HEAD).astype(F32)
        q = unit(swish(block[:, :HEAD])) * HEAD**-0.5
        k = unit(swish(block[:, HEAD : 2 * HEAD]))
        v = swish(block[:, 2 * HEAD :])
        lines = gr[2 * p] + gr[2 * p + 1]
        beta_row, gate_row = lines[0:1], lines[1:2]
        beta, gate = upright(beta_row, eye), upright(gate_row, eye)
        last = upright(gate_row, col == (row // BLOCK) * BLOCK + BLOCK - 1)
        decay = jnp.exp(jnp.where(causal, gate - gate_row, 0.0))
        lower = jnp.where(strict, beta * mm_nt(k, k) * decay, 0.0)
        scores = jnp.where(causal, mm_nt(q, k) * decay, 0.0)
        inverse = jnp.where(eye, 1.0, 0.0) - jnp.where((row // 2 == col // 2), lower, 0.0)
        width = 2
        while width < BLOCK:
            pick = (row // (2 * width) == col // (2 * width)) & (row // width != col // width)
            inverse = inverse - mm(mm(inverse, jnp.where(pick, lower, 0.0)), inverse)
            width *= 2
        both = mm(inverse, jnp.concatenate([beta * v, beta * k * jnp.exp(gate)], axis=1))
        key_t = (k * jnp.exp(last - gate)).T
        moves = [
            mm(key_t, jnp.where(wide_row // BLOCK == h, both, 0.0)) for h in range(2)
        ]
        factors = [jnp.exp(last[h * BLOCK : h * BLOCK + 1]) for h in range(2)]
        terms.append((q * jnp.exp(gate), scores, both, moves, factors))

    total = jnp.concatenate([jnp.zeros((size, size), F32), jnp.where(eye, 1.0, 0.0)], axis=1)
    states = []
    for j in range(half):
        states.append(total)
        move, factor = terms[j // 2][3][j % 2], terms[j // 2][4][j % 2]
        grown = factor * total - mm(move[:, size:], total)
        total = jnp.concatenate([grown[:, :size] + move[:, :size], grown[:, size:]], axis=1)

    state_out[...] = total[:, :size]
    crossing = remote(state_out, state_in, st_send.at[0], st_recv.at[0], partner)

    @pl.when(t == 0)
    def _():
        state_in[...] = jnp.zeros_like(state_in)
        crossing.start()

    @pl.when(t == 1)
    def _():
        crossing.wait_recv()

    start = state_in[...]
    for p in range(half // 2):
        queries, scores, both, _, _ = terms[p]
        read, fixed = [], []
        for h in range(2):
            j = 2 * p + h
            state = states[j][:, :size] + mm(states[j][:, size:], start)
            cut = slice(h * BLOCK, (h + 1) * BLOCK)
            got = mm(jnp.concatenate([both[cut, size:], queries[cut]], axis=0), state)
            fixed.append(both[cut, :size] - got[:BLOCK])
            read.append(got[BLOCK:])
        raw = jnp.concatenate(read, axis=0) + mm(scores, jnp.concatenate(fixed, axis=0))
        raw = raw * lax.rsqrt(jnp.mean(raw * raw, axis=-1, keepdims=True) + NORM_EPS)
        done = (raw * dgain_ref[...]).astype(BF16)
        ready[2 * p] = done[:BLOCK]
        ready[2 * p + 1] = done[BLOCK:]

    for i in range(half):
        j = lax.rem(zl + i, half)
        begin(
            remote(
                ready.at[j],
                homed.at[lax.rem(zl, 2), x],
                h_send.at[i],
                h_recv.at[lax.rem(zl, 2), x],
                {"fs": zl // 2, "sp": half * t + j, "tp": lane_t},
            )
        )

    for k in range(nz - 1):
        slot = kvg.at[1 - t, lax.rem(z + 1, nz)]
        remote(slot, slot, kp_send.at[k], kp_recv.at[k], partner).wait_recv()
    allowed = lax.broadcasted_iota(jnp.int32, (1, nz * BLOCK), 1) < (z + 1) * BLOCK
    outs = []
    low = lax.broadcasted_iota(jnp.int32, (BLOCK, LANES), 1) < LANES // 2
    for s in range(count):
        keys = kvg[s].reshape(nz * BLOCK, kvg.shape[3])
        scores = mm_nt(jnp.concatenate(stacked[s], axis=0), keys) * (NOPE + ROPE) ** (-0.5)
        scores = jnp.where(allowed, scores, -1e30)
        peak = jnp.max(scores, axis=-1, keepdims=True)
        weights = jnp.where(allowed, jnp.exp(scores - peak), 0.0)
        total = jnp.sum(weights, axis=-1, keepdims=True)
        mixed = (mm(weights, keys[:, :kv_total]) / total).astype(BF16)
        made = [
            mm(mixed[h * BLOCK : (h + 1) * BLOCK], lup_ref[:, h * LANES : (h + 1) * LANES])
            for h in range(heads)
        ]
        pairs = [
            jnp.where(low, pltpu.roll(made[h], LANES // 2, 1), made[h + 1]).astype(BF16)
            for h in range(0, heads, 2)
        ]
        outs.append(jnp.concatenate(pairs, axis=1))
    latent_heads = jnp.concatenate(outs, axis=0)

    own_c.wait()
    for k, owner, upper in (
        (2, lax.rem(x + nx - 1, nx), 1),
        (3, lax.rem(x + 1, nx), 0),
        (4, lax.rem(x + 2, nx), 0),
        (5, lax.rem(x + 2, nx), 1),
    ):
        remote(
            w_part(owner, upper), w_part(owner, upper), w_send.at[k], w_recv.at[k], east
        ).wait_recv()
    for sl in range(2):
        for xl in range(nx):
            slot = homed.at[sl, xl]
            where = {"fs": xl, "sp": 2 * x + sl + half * (1 - t), "tp": zh}
            remote(slot, slot, h_send.at[0], h_recv.at[sl, xl], where).wait_recv()
    delta_heads = [homed[:, xl].reshape(rows, HEAD) for xl in range(nx)]
    joined = jnp.concatenate(delta_heads + [latent_heads], axis=1)
    width = wo.shape[0] * wo.shape[1] * wo.shape[2]
    columns = wo[...].reshape(width, wo.shape[3])
    part_out[...] = mm_nt(joined, columns).astype(BF16)
    swap_parts = begin(remote(part_out, part_in, p_send.at[0], p_recv.at[0], partner))
    swap_parts.wait_recv()
    whole = part_out[...].astype(F32) + part_in[...].astype(F32)
    scale = lax.rsqrt(jnp.mean(whole * whole, axis=-1, keepdims=True) + NORM_EPS)
    own_half = jnp.where(t == 0, whole[:, : width // 2], whole[:, width // 2 :])
    out_ref[...] = (own_half * scale * post_ref[...]).astype(BF16)

    for copy in started:
        copy.wait_send()

    def drain(step, carry):
        for part in [*range(nx), None]:
            go_right(step, part, z).wait_send()

            @pl.when(step < reach_l)
            def _():
                go_left(step, part, z).wait_send()

        return carry

    lax.fori_loop(0, reach_r, drain, 0)

    @pl.when(t == 0)
    def _():
        crossing.wait_send()


def layer(nz, nx, *operands):
    tokens, query_weight, out_cols, latent_up = (operands[k] for k in (0, 2, 9, 13))
    half = nz // 2
    seqs, length, width = tokens.shape
    rows = seqs * length
    span = query_weight.shape[0]
    slab = latent_up.shape[0] + LANES
    dma = pltpu.SemaphoreType.DMA

    def pair(*shape):
        return [dma(shape), dma(shape)]

    specs = [pl.BlockSpec(memory_space=VM)] * len(operands)
    specs[8] = pl.BlockSpec(memory_space=pltpu.SMEM)
    return pl.pallas_call(
        functools.partial(layer_kernel, nz, nx),
        out_shape=jax.ShapeDtypeStruct((rows, width // 2), BF16),
        in_specs=specs,
        out_specs=pl.BlockSpec(memory_space=VM),
        scratch_shapes=[
            VM((seqs * nx, length, width), BF16),
            VM((nx * rows, width), BF16),
            VM((nz, nx * span, 4 * LANES), BF16),
            VM((nz, *out_cols.shape), BF16),
            VM((nx, span, LANES), BF16),
            VM((nx * rows, 4 * LANES), F32),
            VM((2 * nx, LANES, 4 * LANES), BF16),
            VM((half, BLOCK, 3 * HEAD), BF16),
            VM((half, 8, LANES), F32),
            VM((nx, rows, LANES), BF16),
            VM((half, BLOCK, 3 * HEAD), BF16),
            VM((half, 8, LANES), F32),
            VM((2 * nx, rows, LANES), BF16),
            VM((seqs, nz, length, slab), BF16),
            VM((nz, nx, *out_cols.shape), BF16),
            VM((2, nx, BLOCK, HEAD), BF16),
            VM((half, BLOCK, HEAD), BF16),
            VM((HEAD, HEAD), F32),
            VM((HEAD, HEAD), F32),
            VM((rows, width), BF16),
            VM((rows, width), BF16),
            dma((6,)),
            *pair(nx - 1, 4),
            *pair(nx - 1),
            *pair(nx - 1),
            *pair(half, nx + 1),
            *pair(half - 1, nx + 1),
            *pair(2 * nx - 1),
            *pair(half),
            *pair(half),
            *pair(half),
            *pair(half - 1),
            *pair(nz - 1),
            *pair(6),
            *pair(1),
            dma((half,)),
            dma((2, nx)),
            *pair(1),
        ],
        compiler_params=pltpu.CompilerParams(collective_id=1, has_side_effects=True),
        name="layer",
    )(*operands)


def rope_tables(count, length):
    frequency = ROPE_THETA ** (-np.arange(0, ROPE, 2, dtype=np.float64) / ROPE)
    frequency = np.tile(frequency, LANES // (ROPE // 2))[None, :]

    def both(positions):
        angles = positions[:, None] * frequency
        return np.stack([np.cos(angles), np.sin(angles)]).astype(np.float32)

    return both(np.arange(count) * float(length)), both(np.arange(length) * 1.0)


def local(
    tokens,
    pre_gain,
    query_weight,
    key_weight,
    value_weight,
    beta_weight,
    decay_weight,
    decay_rate,
    delta_gain,
    query_down,
    latent_down,
    rope_weight,
    query_gain,
    latent_gain,
    query_up,
    latent_up,
    delta_out,
    latent_out,
    post_gain,
):
    nz, nx = lax.axis_size("sp"), lax.axis_size("fs")
    z, x = lax.axis_index("sp"), lax.axis_index("fs")
    seq_count, token_count = tokens.shape[:2]
    span = query_weight.shape[0]
    small = jnp.concatenate(
        [
            lax.dynamic_slice_in_dim(array, (z * nx + x) * span, span, 0)
            for array in (rope_weight, beta_weight, decay_weight)
        ],
        axis=1,
    )
    small = jnp.pad(small, ((0, 0), (0, LANES - small.shape[1])))
    out_cols = jnp.concatenate([delta_out, latent_out], axis=0).T
    far, near = rope_tables(nz, token_count)
    result = layer(
        nz,
        nx,
        tokens,
        pre_gain[None],
        query_weight,
        key_weight,
        value_weight,
        query_down,
        latent_down,
        small,
        decay_rate,
        out_cols,
        query_gain[None],
        latent_gain[None],
        query_up,
        latent_up,
        jnp.asarray(far),
        jnp.asarray(near),
        delta_gain[None],
        post_gain[None],
    )
    return result.reshape(seq_count, token_count, result.shape[1])


def solution(mesh):
    return jax.shard_map(
        local,
        mesh=mesh,
        in_specs=(
            P(("grp", "fs"), "sp", None),
            P(),
            P(("sp", "fs"), "tp"),
            P(("sp", "fs"), "tp"),
            P(("sp", "fs"), "tp"),
            P(),
            P(),
            P(),
            P(),
            P(("sp", "fs"), None),
            P(("sp", "fs"), None),
            P(),
            P(),
            P(),
            P(None, "tp"),
            P(None, "tp"),
            P("tp", ("sp", "fs")),
            P("tp", ("sp", "fs")),
            P("tp"),
        ),
        out_specs=P(("grp", "fs"), "sp", "tp"),
        check_vma=False,
    )
```

time: 176 us -> 143 us (0.81)
  local copies, waits for them, and re-layouts: 17.5 us -> 2.86 us
  other arithmetic: 9.7 us -> 1.32 us
  Pallas kernels: 147 us -> 139 us
    pallas_call x2 -> x1, Pallas kernels: 147 us -> 139 us  [layer(): pl.pallas_call(functools.partial(layer_kernel, nz, nx), out_shape=jax.Sha...]
    reshape x6 -> x0, local copies, waits for them, and re-layouts: 3.4 us -> none  [the longest x2 1.69 us: for_cores(): parts = array.reshape(row_span, nx, 2, -1)]
    another operation x8 -> x0, local copies, waits for them, and re-layouts: 2.79 us -> none  [the longest x6 1.77 us: local(): jnp.tile(table, (seq_count, LANES // (ROPE // 2)))]
    concatenate x7 -> x0, local copies, waits for them, and re-layouts: 2.57 us -> none  [the longest x6 2.45 us: local(): jnp.concatenate([u.reshape(u.shape[0], -1) for u in (up[..., :NOPE], turn...]
    slice x5 -> x0, local copies, waits for them, and re-layouts: 2.27 us -> none  [the longest x1 0.81 us: local(): projected[:, :3 * HEAD].astype(jnp.bfloat16)]
where the time goes in v3:
time: 143 us
  Pallas kernels  139 us (97%)
  local copies, waits for them, and re-layouts  2.86 us (2%)
    pallas_call x1, Pallas kernels, layer(): pl.pallas_call(functools.partial(layer_kernel, nz, nx), out_shape=jax.Sha...  139 us

profile of v3, /device:TPU:33, one launch (start us, length us, event | category | flops | bytes accessed | tf_op | source)
XLA Modules:
  0.0 142.9 jit_solution(9191199692562654919)
XLA Ops:
  0.0 0.0 copy-start
  0.0 0.8 constant_dynamic-slice_fusion
  0.8 0.1 copy.27
  0.9 0.0 copy-done
  0.9 0.0 copy-start.2
  0.9 0.1 constant_dynamic-slice_fusion.2
  1.0 0.0 copy-start.1
  1.0 0.1 copy.25
  1.1 0.1 copy.26
  1.2 0.7 fusion.4.small_ref
  1.9 0.0 copy-done.2
  1.9 0.0 copy-done.1
  1.9 0.6 maximum_bitcast_fusion.wt_ref
  2.5 138.7 %layer.1 = bf16[128,1024]{1,0:T(8,128)(2,1)} custom-call(bf16[2,64,2048]{2,1,0:T(8,128)(2,1)} %tok_ref.1, f32[1,2048]{1,0:T(1,128)} %bitcast.9, bf16[32,512]{1,0:T(8,128)(2,1)} %wq_ref.1, bf16[32,512]{1,0:T(8,128)(2,1)} %wk_ref.1, bf16[32,512]{1,0:T(8,128)(2,1)} %wv_ref.1, bf16[32,512]{1,0:T(8,128)(2,1)} %qd_ref.1, bf16[32,256]{1,0:T(8,128)(2,1)} %kvd_ref.1, ...), custom_call_target="tpu_custom_call" | custom-call | tf_op jit(solution)/shard_map/layer/pallas_call | solution.py:584
  141.2 1.7 %copy.29 = bf16[2,64,1024]{2,1,0:T(8,128)(2,1)} copy(bf16[2,64,1024]{2,1,0:T(8,128)(2,1)} %bitcast.8) | data formatting | bytes 524288
Async XLA Ops:
  0.0 0.9 copy-start
  0.9 0.9 copy-start.2
  1.0 0.9 copy-start.1

commit v4 on v3

--- a/solution.py
+++ b/solution.py
@@ -89,7 +89,7 @@
     right, left = {"sp": lax.rem(z + 1, nz)}, {"sp": lax.rem(z + nz - 1, nz)}
     east, west = {"fs": lax.rem(x + 1, nx)}, {"fs": lax.rem(x + nx - 1, nx)}
     sources = [{"fs": back, "tp": to} for dx, dt, fx, to, back in near]
-    sources += [right, left]
+    sources += [{"sp": lax.rem(z + hop, nz)} for hop in (1, 2, nz - 2, nz - 1)]
     sources += [{"sp": half * t + j, "tp": 1 - zh} for j in range(half)]
     sources += [
         {"fs": xl, "sp": 2 * x + sl + half * (1 - t), "tp": zh} for sl in range(2) for xl in range(nx)
@@ -127,6 +127,24 @@
     own_w = [local(columns_of(ref, x), piece(k), k) for k, ref in enumerate(mains)]
     own_o = local(wt_ref, wz.at[z], 3)
     own_t = local(tok_ref, toks.at[pl.ds(2 * x, 2)], 4)
+
+    reach_r, reach_l = nz // 2, nz // 2 - 1
+
+    def go_right(step, part, slot):
+        mark = nx if part is None else part
+        return remote(
+            chunk(slot, part), chunk(slot, part), r_send.at[step, mark], r_recv.at[step, mark], right
+        )
+
+    def go_left(step, part, slot):
+        mark = nx if part is None else part
+        return remote(
+            chunk(slot, part), chunk(slot, part), l_send.at[step, mark], l_recv.at[step, mark], left
+        )
+
+    own_o.wait()
+    go_right(0, None, z).start()
+    go_left(0, None, z).start()
 
     q_width, kv_width = qd_ref.shape[1] // cores, kvd_ref.shape[1] // cores
     rope_width = ROPE // cores
@@ -162,20 +180,6 @@
     for d, o in enumerate(others):
         begin(remote(tok_ref.at[t], toks.at[2 * x + t], tok_send.at[d], tok_recv.at[d], {"fs": o}))
 
-    reach_r, reach_l = nz // 2, nz // 2 - 1
-
-    def go_right(step, part, slot):
-        mark = nx if part is None else part
-        return remote(
-            chunk(slot, part), chunk(slot, part), r_send.at[step, mark], r_recv.at[step, mark], right
-        )
-
-    def go_left(step, part, slot):
-        mark = nx if part is None else part
-        return remote(
-            chunk(slot, part), chunk(slot, part), l_send.at[step, mark], l_recv.at[step, mark], left
-        )
-
     for d in range(nx):
         part = lax.rem(x + nx - d, nx)
         if d == 0:
@@ -188,9 +192,6 @@
                 ).wait_recv()
         go_right(0, part, z).start()
         go_left(0, part, z).start()
-    own_o.wait()
-    go_right(0, None, z).start()
-    go_left(0, None, z).start()
 
     from_lane = lax.broadcasted_iota(jnp.int32, (LANES, 4 * LANES), 0)
     to_lane = lax.broadcasted_iota(jnp.int32, (LANES, 4 * LANES), 1)
@@ -210,8 +211,8 @@
     def ring(step, carry):
         from_left = lax.rem(z + 2 * nz - 1 - step, nz)
         from_right = lax.rem(z + 1 + step, nz)
-        for d in range(nx + 1):
-            part = lax.rem(x + nx - d, nx) if d < nx else None
+        for d in range(-1, nx):
+            part = lax.rem(x + nx - d, nx) if d >= 0 else None
             go_right(step, part, from_left).wait_recv()
 
             @pl.when(step < reach_r - 1)
@@ -290,8 +291,8 @@
     same = (row // BLOCK) == (col // BLOCK)
     rate = rate_ref[nx * t + x]
     even = lax.rem(z, 2) == 0
-    line = lax.broadcasted_iota(jnp.int32, (8, LANES), 0)
-    first_half = lax.broadcasted_iota(jnp.int32, (8, LANES), 1) < LANES // 2
+    line = lax.broadcasted_iota(jnp.int32, (2, LANES), 0)
+    first_half = lax.broadcasted_iota(jnp.int32, (2, LANES), 1) < LANES // 2
     for p in range(half // 2):
         blocks[2 * p : 2 * p + 2] = (
             proj[p * size : (p + 1) * size, : 3 * HEAD].astype(BF16).reshape(2, BLOCK, 3 * HEAD)
@@ -302,7 +303,7 @@
         fade = -rate * (jnp.maximum(pushed, 0.0) + jnp.log1p(jnp.exp(-jnp.abs(pushed))))
         write_row = jnp.sum(jnp.where(eye, write, 0.0), axis=0, keepdims=True)
         fade_row = jnp.sum(jnp.where(same & (row <= col), fade, 0.0), axis=0, keepdims=True)
-        both_rows = jnp.where(line == 0, write_row, jnp.where(line == 1, fade_row, 0.0))
+        both_rows = jnp.where(line == 0, write_row, fade_row)
         rolled = pltpu.roll(both_rows, LANES // 2, 1)
         lines_out[2 * p] = jnp.where(
             even, jnp.where(first_half, both_rows, 0.0), jnp.where(first_half, 0.0, rolled)
@@ -337,21 +338,36 @@
     kv_lat = slab[:, :kv_total]
     kv_lat = kv_lat * lax.rsqrt(jnp.mean(kv_lat * kv_lat, axis=-1, keepdims=True) + NORM_EPS)
     turned = slab[:, kv_total : kv_total + LANES] * cosine + slab[:, kv_total + LANES :] * sine
-    keys = jnp.concatenate([kv_lat * kvgain_ref[...], turned], axis=1).astype(BF16)
+    latent_keys = (kv_lat * kvgain_ref[...]).astype(BF16)
+    groups = LANES // ROPE
+    short = BLOCK // groups
+    in_group = lax.broadcasted_iota(jnp.int32, (short, LANES), 1) // ROPE
     for s in range(count):
-        kvg[s, z] = keys[s * BLOCK : (s + 1) * BLOCK]
-
-    def key_right(step, slot):
-        return remote(kvg.at[t, slot], kvg.at[t, slot], kr_send.at[step], kr_recv.at[step], right)
-
-    def key_left(step, slot):
-        return remote(kvg.at[t, slot], kvg.at[t, slot], kl_send.at[step], kl_recv.at[step], left)
+        kvg[s, z, 0:BLOCK] = latent_keys[s * BLOCK : (s + 1) * BLOCK]
+        tight = jnp.zeros((short, LANES), F32)
+        for g in range(groups):
+            at = s * BLOCK + g * short
+            tight = jnp.where(in_group == g, turned[at : at + short], tight)
+        kvg[s, z, BLOCK : BLOCK + short] = jnp.concatenate(
+            [tight, jnp.zeros((short, kv_total - LANES), F32)], axis=1
+        ).astype(BF16)
+
+    def key_right(distance, slot):
+        hop = 2 - distance % 2
+        sems = kr_send.at[distance - 1], kr_recv.at[distance - 1]
+        return remote(kvg.at[t, slot], kvg.at[t, slot], *sems, {"sp": lax.rem(z + hop, nz)})
+
+    def key_left(distance, slot):
+        hop = 2 - distance % 2
+        sems = kl_send.at[distance - 1], kl_recv.at[distance - 1]
+        return remote(kvg.at[t, slot], kvg.at[t, slot], *sems, {"sp": lax.rem(z + nz - hop, nz)})
 
     def across(slot, k):
         return remote(kvg.at[t, slot], kvg.at[t, slot], kp_send.at[k], kp_recv.at[k], partner)
 
-    begin(key_right(0, z))
-    begin(key_left(0, z))
+    for distance in (2, 1):
+        begin(key_right(distance, z))
+        begin(key_left(distance, z))
 
     q_lat = jnp.concatenate(
         [
@@ -368,12 +384,10 @@
     query = mm(q_lat * qgain_ref[...], qup_ref[...]).astype(BF16).astype(F32)
     head_width = NOPE + ROPE
     heads = query.shape[1] // head_width
-    is_turn = (lane >= NOPE) & (lane < head_width)
-    from_turn = (row >= NOPE) & (row < head_width)
-    low_turn = (col >= NOPE) & (col < NOPE + ROPE // 2)
-    high_turn = (col >= NOPE + ROPE // 2) & (col < head_width)
-    exchange = jnp.where(from_turn & high_turn & (row == col - ROPE // 2), 1.0, 0.0)
-    exchange = exchange - jnp.where(from_turn & low_turn & (row == col + ROPE // 2), 1.0, 0.0)
+    entry = lax.rem(col, ROPE)
+    repeat = ones(row == NOPE + entry)
+    exchange = jnp.where((entry >= ROPE // 2) & (row == NOPE + entry - ROPE // 2), 1.0, 0.0)
+    exchange = exchange - ones((entry < ROPE // 2) & (row == NOPE + entry + ROPE // 2))
     stacked = [[] for _ in range(count)]
     for h in range(heads):
         own = query[:, h * head_width : (h + 1) * head_width]
@@ -381,31 +395,37 @@
         absorbed = mm_nt(
             jnp.where(lane < NOPE, own, 0.0), lup_ref[:, h * LANES : (h + 1) * LANES]
         )
-        turn = jnp.where(is_turn, own * cosine + mm(own, exchange) * sine, 0.0)
+        turn = mm(own, repeat) * cosine + mm(own, exchange) * sine
         joined = jnp.concatenate([absorbed, turn], axis=1).astype(BF16)
         for s in range(count):
             stacked[s].append(joined[s * BLOCK : (s + 1) * BLOCK])
 
-    for step in range(reach_r):
-        if step + 2 < half:
-            send_lane(step + 2)
-        from_left = lax.rem(z + 2 * nz - 1 - step, nz)
-        from_right = lax.rem(z + 1 + step, nz)
-        key_right(step, from_left).wait_recv()
-        if step < reach_r - 1:
-            begin(key_right(step + 1, from_left))
-        begin(across(from_left, step))
-        if step < reach_l:
-            key_left(step, from_right).wait_recv()
-            if step < reach_l - 1:
-                begin(key_left(step + 1, from_right))
-            begin(across(from_right, reach_r + step))
-
-    behind, ahead = lax.rem(x + nx - 1, nx), lax.rem(x + 1, nx)
-    remote(w_part(behind, 0), w_part(behind, 0), w_send.at[0], w_recv.at[0], west).wait_recv()
-    begin(remote(w_part(behind, 0), w_part(behind, 0), w_send.at[4], w_recv.at[4], east))
-    remote(w_part(ahead, 1), w_part(ahead, 1), w_send.at[1], w_recv.at[1], east).wait_recv()
-    begin(remote(w_part(ahead, 1), w_part(ahead, 1), w_send.at[5], w_recv.at[5], west))
+    for turn_at in range(reach_r // 2):
+        for i in (2 * turn_at + 2, 2 * turn_at + 3):
+            if i < half:
+                send_lane(i)
+        for distance in (2 * turn_at + 2, 2 * turn_at + 1):
+            from_left = lax.rem(z + nz - distance, nz)
+            from_right = lax.rem(z + distance, nz)
+            key_right(distance, from_left).wait_recv()
+            if distance % 2 == 0:
+                for further in (distance + 2, distance + 1):
+                    if further <= reach_r:
+                        begin(key_right(further, from_left))
+            begin(across(from_left, distance - 1))
+            if distance <= reach_l:
+                key_left(distance, from_right).wait_recv()
+                if distance % 2 == 0:
+                    for further in (distance + 2, distance + 1):
+                        if further <= reach_l:
+                            begin(key_left(further, from_right))
+                begin(across(from_right, reach_r + distance - 1))
+        if turn_at == reach_r // 2 - 2:
+            behind, ahead = lax.rem(x + nx - 1, nx), lax.rem(x + 1, nx)
+            remote(w_part(behind, 0), w_part(behind, 0), w_send.at[0], w_recv.at[0], west).wait_recv()
+            begin(remote(w_part(behind, 0), w_part(behind, 0), w_send.at[4], w_recv.at[4], east))
+            remote(w_part(ahead, 1), w_part(ahead, 1), w_send.at[1], w_recv.at[1], east).wait_recv()
+            begin(remote(w_part(ahead, 1), w_part(ahead, 1), w_send.at[5], w_recv.at[5], west))
 
     for j in range(half):
         where = {"sp": half * t + j, "tp": 1 - zh}
@@ -419,32 +439,55 @@
     def upright(line, where):
         return jnp.sum(jnp.where(where, line, 0.0), axis=1, keepdims=True)
 
-    terms = []
-    for p in range(half // 2):
-        block = dr[2 * p : 2 * p + 2].reshape(size, 3 * HEAD).astype(F32)
-        q = unit(swish(block[:, :HEAD])) * HEAD**-0.5
-        k = unit(swish(block[:, HEAD : 2 * HEAD]))
-        v = swish(block[:, 2 * HEAD :])
-        lines = gr[2 * p] + gr[2 * p + 1]
-        beta_row, gate_row = lines[0:1], lines[1:2]
-        beta, gate = upright(beta_row, eye), upright(gate_row, eye)
-        last = upright(gate_row, col == (row // BLOCK) * BLOCK + BLOCK - 1)
-        decay = jnp.exp(jnp.where(causal, gate - gate_row, 0.0))
-        lower = jnp.where(strict, beta * mm_nt(k, k) * decay, 0.0)
-        scores = jnp.where(causal, mm_nt(q, k) * decay, 0.0)
-        inverse = jnp.where(eye, 1.0, 0.0) - jnp.where((row // 2 == col // 2), lower, 0.0)
-        width = 2
-        while width < BLOCK:
-            pick = (row // (2 * width) == col // (2 * width)) & (row // width != col // width)
-            inverse = inverse - mm(mm(inverse, jnp.where(pick, lower, 0.0)), inverse)
-            width *= 2
-        both = mm(inverse, jnp.concatenate([beta * v, beta * k * jnp.exp(gate)], axis=1))
-        key_t = (k * jnp.exp(last - gate)).T
-        moves = [
-            mm(key_t, jnp.where(wide_row // BLOCK == h, both, 0.0)) for h in range(2)
-        ]
-        factors = [jnp.exp(last[h * BLOCK : h * BLOCK + 1]) for h in range(2)]
-        terms.append((q * jnp.exp(gate), scores, both, moves, factors))
+    pairs_at = range(half // 2)
+    raws = [dr[2 * p : 2 * p + 2].reshape(size, 3 * HEAD).astype(F32) for p in pairs_at]
+    qs = [unit(swish(raw[:, :HEAD])) * HEAD**-0.5 for raw in raws]
+    ks = [unit(swish(raw[:, HEAD : 2 * HEAD])) for raw in raws]
+    vs = [swish(raw[:, 2 * HEAD :]) for raw in raws]
+    marks = [gr[2 * p] + gr[2 * p + 1] for p in pairs_at]
+    betas = [upright(mark[0:1], eye) for mark in marks]
+    sums = [upright(mark[1:2], eye) for mark in marks]
+    ends = [
+        upright(mark[1:2], col == (row // BLOCK) * BLOCK + BLOCK - 1) for mark in marks
+    ]
+    decays = [
+        jnp.exp(jnp.where(causal, upon - mark[1:2], 0.0)) for upon, mark in zip(sums, marks)
+    ]
+    lowers = [
+        jnp.where(strict, beta * mm_nt(k, k) * decay, 0.0)
+        for beta, k, decay in zip(betas, ks, decays)
+    ]
+    inverses = [
+        jnp.where(eye, 1.0, 0.0) - jnp.where((row // 2 == col // 2), low, 0.0) for low in lowers
+    ]
+    level = 2
+    while level < BLOCK:
+        pick = (row // (2 * level) == col // (2 * level)) & (row // level != col // level)
+        firsts = [mm(inv, jnp.where(pick, low, 0.0)) for inv, low in zip(inverses, lowers)]
+        inverses = [inv - mm(first, inv) for first, inv in zip(firsts, inverses)]
+        level *= 2
+    scores_of = [
+        jnp.where(causal, mm_nt(q, k) * decay, 0.0) for q, k, decay in zip(qs, ks, decays)
+    ]
+    boths = [
+        mm(inv, jnp.concatenate([beta * v, beta * k * jnp.exp(upon)], axis=1))
+        for inv, beta, v, k, upon in zip(inverses, betas, vs, ks, sums)
+    ]
+    keys_t = [(k * jnp.exp(end - upon)).T for k, end, upon in zip(ks, ends, sums)]
+    moves_of = [
+        [mm(key_t, jnp.where(wide_row // BLOCK == h, both, 0.0)) for h in range(2)]
+        for key_t, both in zip(keys_t, boths)
+    ]
+    terms = [
+        (
+            qs[p] * jnp.exp(sums[p]),
+            scores_of[p],
+            boths[p],
+            moves_of[p],
+            [jnp.exp(ends[p][h * BLOCK : h * BLOCK + 1]) for h in range(2)],
+        )
+        for p in pairs_at
+    ]
 
     total = jnp.concatenate([jnp.zeros((size, size), F32), jnp.where(eye, 1.0, 0.0)], axis=1)
     states = []
@@ -499,10 +542,19 @@
         slot = kvg.at[1 - t, lax.rem(z + 1, nz)]
         remote(slot, slot, kp_send.at[k], kp_recv.at[k], partner).wait_recv()
     allowed = lax.broadcasted_iota(jnp.int32, (1, nz * BLOCK), 1) < (z + 1) * BLOCK
+    rope_group = lax.broadcasted_iota(jnp.int32, (nz, short, LANES), 2) // ROPE
     outs = []
     low = lax.broadcasted_iota(jnp.int32, (BLOCK, LANES), 1) < LANES // 2
     for s in range(count):
-        keys = kvg[s].reshape(nz * BLOCK, kvg.shape[3])
+        tight = kvg[s, :, BLOCK : BLOCK + short, :LANES].astype(F32)
+        spread = [jnp.where(rope_group == g, tight, 0.0) for g in range(groups)]
+        keys = jnp.concatenate(
+            [
+                kvg[s, :, 0:BLOCK, :].reshape(nz * BLOCK, kv_total),
+                jnp.concatenate(spread, axis=1).reshape(nz * BLOCK, LANES).astype(BF16),
+            ],
+            axis=1,
+        )
         scores = mm_nt(jnp.concatenate(stacked[s], axis=0), keys) * (NOPE + ROPE) ** (-0.5)
         scores = jnp.where(allowed, scores, -1e30)
         peak = jnp.max(scores, axis=-1, keepdims=True)
@@ -573,7 +625,6 @@
     seqs, length, width = tokens.shape
     rows = seqs * length
     span = query_weight.shape[0]
-    slab = latent_up.shape[0] + LANES
     dma = pltpu.SemaphoreType.DMA
 
     def pair(*shape):
@@ -595,12 +646,12 @@
             VM((nx * rows, 4 * LANES), F32),
             VM((2 * nx, LANES, 4 * LANES), BF16),
             VM((half, BLOCK, 3 * HEAD), BF16),
-            VM((half, 8, LANES), F32),
+            VM((half, 2, LANES), F32),
             VM((nx, rows, LANES), BF16),
             VM((half, BLOCK, 3 * HEAD), BF16),
-            VM((half, 8, LANES), F32),
+            VM((half, 2, LANES), F32),
             VM((2 * nx, rows, LANES), BF16),
-            VM((seqs, nz, length, slab), BF16),
+            VM((seqs, nz, length + length * ROPE // LANES, latent_up.shape[0]), BF16),
             VM((nz, nx, *out_cols.shape), BF16),
             VM((2, nx, BLOCK, HEAD), BF16),
             VM((half, BLOCK, HEAD), BF16),

time: 143 us -> 129 us (0.902)
  Pallas kernels: 139 us -> 125 us
    pallas_call x1, Pallas kernels: 139 us -> 125 us  [layer(): pl.pallas_call(functools.partial(layer_kernel, nz, nx), out_shape=jax.Sha...]
where the time goes in v4:
time: 129 us
  Pallas kernels  125 us (97%)
  local copies, waits for them, and re-layouts  2.86 us (2%)
  other arithmetic  1.32 us (1%)
    pallas_call x1, Pallas kernels, layer(): pl.pallas_call(functools.partial(layer_kernel, nz, nx), out_shape=jax.Sha...  125 us

profile of v4, /device:TPU:33, one launch (start us, length us, event | category | flops | bytes accessed | tf_op | source)
XLA Modules:
  0.0 129.2 jit_solution(15288676437764803570)
XLA Ops:
  0.0 0.0 copy-start
  0.0 0.8 constant_dynamic-slice_fusion
  0.8 0.1 copy.27
  0.9 0.0 copy-done
  0.9 0.0 copy-start.2
  0.9 0.1 constant_dynamic-slice_fusion.2
  1.0 0.0 copy-start.1
  1.0 0.1 copy.25
  1.1 0.1 copy.26
  1.2 0.7 fusion.4.small_ref
  1.9 0.0 copy-done.2
  1.9 0.0 copy-done.1
  1.9 0.6 maximum_bitcast_fusion.wt_ref
  2.5 125.0 %layer.1 = bf16[128,1024]{1,0:T(8,128)(2,1)} custom-call(bf16[2,64,2048]{2,1,0:T(8,128)(2,1)} %tok_ref.1, f32[1,2048]{1,0:T(1,128)} %bitcast.9, bf16[32,512]{1,0:T(8,128)(2,1)} %wq_ref.1, bf16[32,512]{1,0:T(8,128)(2,1)} %wk_ref.1, bf16[32,512]{1,0:T(8,128)(2,1)} %wv_ref.1, bf16[32,512]{1,0:T(8,128)(2,1)} %qd_ref.1, bf16[32,256]{1,0:T(8,128)(2,1)} %kvd_ref.1, ...), custom_call_target="tpu_custom_call" | custom-call | tf_op jit(solution)/shard_map/layer/pallas_call | solution.py:635
  127.5 1.7 %copy.29 = bf16[2,64,1024]{2,1,0:T(8,128)(2,1)} copy(bf16[2,64,1024]{2,1,0:T(8,128)(2,1)} %bitcast.8) | data formatting | bytes 524288
Async XLA Ops:
  0.0 0.9 copy-start
  0.9 0.9 copy-start.2
  1.0 0.9 copy-start.1

commit v5 on v4

--- a/solution.py
+++ b/solution.py
@@ -68,7 +68,7 @@
     dr, gr, lr, kvg, wo, homed, ready, state_out, state_in, part_out, part_in,
     loc_sem, wx_send, wx_recv, tok_send, tok_recv, fwd_send, fwd_recv, r_send, r_recv, l_send, l_recv,
     a_send, a_recv, d_send, d_recv, g_send, g_recv, kr_send, kr_recv, kl_send, kl_recv,
-    kp_send, kp_recv, w_send, w_recv, st_send, st_recv, h_send, h_recv, p_send, p_recv,
+    kp_send, kp_recv, w_send, w_recv, v_send, v_recv, st_send, st_recv, h_send, h_recv, p_send, p_recv,
 ):
     z, x, t = lax.axis_index("sp"), lax.axis_index("fs"), lax.axis_index("tp")
     half = nz // 2
@@ -208,11 +208,36 @@
         swapped = is_rope & (spot >= LANES) & (lax.rem(spot_in + ROPE // 2, ROPE) == entry)
         place[c] = (ones(kept | straight) + jnp.where(swapped, sign, 0.0)).astype(BF16)
 
-    def ring(step, carry):
+    early = (reach_r * 5) // 8
+
+    def columns_on(slot):
+        for k, where in enumerate((east, west)):
+            remote(wz.at[slot], wo.at[slot, x], w_send.at[k, slot], w_recv.at[k, slot], where).start()
+
+    def columns_step(step):
         from_left = lax.rem(z + 2 * nz - 1 - step, nz)
         from_right = lax.rem(z + 1 + step, nz)
-        for d in range(-1, nx):
-            part = lax.rem(x + nx - d, nx) if d >= 0 else None
+        go_right(step, None, from_left).wait_recv()
+        columns_on(from_left)
+
+        @pl.when(step < reach_r - 1)
+        def _():
+            go_right(step + 1, None, from_left).start()
+
+        @pl.when(step < reach_l)
+        def _():
+            go_left(step, None, from_right).wait_recv()
+            columns_on(from_right)
+
+        @pl.when(step < reach_l - 1)
+        def _():
+            go_left(step + 1, None, from_right).start()
+
+    def weights_step(step):
+        from_left = lax.rem(z + 2 * nz - 1 - step, nz)
+        from_right = lax.rem(z + 1 + step, nz)
+        for d in range(nx):
+            part = lax.rem(x + nx - d, nx)
             go_right(step, part, from_left).wait_recv()
 
             @pl.when(step < reach_r - 1)
@@ -227,9 +252,12 @@
             def _():
                 go_left(step + 1, part, from_right).start()
 
+    def ring(step, carry):
+        columns_step(step)
+        weights_step(step)
         return carry
 
-    early = (reach_r * 5) // 8
+    columns_on(z)
     lax.fori_loop(0, early, ring, 0)
     own_t.wait()
     for d in range(nx - 1):
@@ -277,12 +305,6 @@
 
     def w_part(owner, upper):
         return wo.at[pl.ds(half * upper, half), owner]
-
-    own_c = local(wz, wo.at[:, x], 1)
-    for upper, where, k in ((0, east, 0), (1, west, 1), (1, east, 2), (0, west, 3)):
-        begin(
-            remote(wz.at[pl.ds(half * upper, half)], w_part(x, upper), w_send.at[k], w_recv.at[k], where)
-        )
 
     size = 2 * BLOCK
     row = lax.broadcasted_iota(jnp.int32, (size, size), 0)
@@ -318,8 +340,8 @@
         begin(remote(lines_out.at[s], gr.at[zl], g_send.at[i], g_recv.at[zl], where))
         begin(remote(blocks.at[s], dr.at[zl], d_send.at[i], d_recv.at[zl], where))
 
-    send_lane(0)
-    send_lane(1)
+    for i in range(half):
+        send_lane(i)
 
     for k, (dx, dt, fx, to, back) in enumerate(near):
         slot = lr.at[2 * back + to]
@@ -400,10 +422,18 @@
         for s in range(count):
             stacked[s].append(joined[s * BLOCK : (s + 1) * BLOCK])
 
-    for turn_at in range(reach_r // 2):
-        for i in (2 * turn_at + 2, 2 * turn_at + 3):
-            if i < half:
-                send_lane(i)
+    own_c = local(wz, wo.at[:, x], 1)
+    behind, ahead = lax.rem(x + nx - 1, nx), lax.rem(x + 1, nx)
+
+    def arrived(k, first, owner):
+        def one(slot, carry):
+            held = wo.at[slot, owner]
+            remote(held, held, w_send.at[k, slot], w_recv.at[k, slot], east).wait_recv()
+            return carry
+
+        lax.fori_loop(first, first + half, one, 0)
+
+    def key_turn(turn_at):
         for distance in (2 * turn_at + 2, 2 * turn_at + 1):
             from_left = lax.rem(z + nz - distance, nz)
             from_right = lax.rem(z + distance, nz)
@@ -420,12 +450,12 @@
                         if further <= reach_l:
                             begin(key_left(further, from_right))
                 begin(across(from_right, reach_r + distance - 1))
-        if turn_at == reach_r // 2 - 2:
-            behind, ahead = lax.rem(x + nx - 1, nx), lax.rem(x + 1, nx)
-            remote(w_part(behind, 0), w_part(behind, 0), w_send.at[0], w_recv.at[0], west).wait_recv()
-            begin(remote(w_part(behind, 0), w_part(behind, 0), w_send.at[4], w_recv.at[4], east))
-            remote(w_part(ahead, 1), w_part(ahead, 1), w_send.at[1], w_recv.at[1], east).wait_recv()
-            begin(remote(w_part(ahead, 1), w_part(ahead, 1), w_send.at[5], w_recv.at[5], west))
+
+    key_turn(0)
+    arrived(0, 0, behind)
+    begin(remote(w_part(behind, 0), w_part(behind, 0), v_send.at[0], v_recv.at[0], east))
+    arrived(1, half, ahead)
+    begin(remote(w_part(ahead, 1), w_part(ahead, 1), v_send.at[1], v_recv.at[1], west))
 
     for j in range(half):
         where = {"sp": half * t + j, "tp": 1 - zh}
@@ -489,6 +519,7 @@
         for p in pairs_at
     ]
 
+    key_turn(1)
     total = jnp.concatenate([jnp.zeros((size, size), F32), jnp.where(eye, 1.0, 0.0)], axis=1)
     states = []
     for j in range(half):
@@ -504,6 +535,8 @@
     def _():
         state_in[...] = jnp.zeros_like(state_in)
         crossing.start()
+
+    key_turn(2)
 
     @pl.when(t == 1)
     def _():
@@ -538,6 +571,8 @@
             )
         )
 
+    for turn_at in range(3, reach_r // 2):
+        key_turn(turn_at)
     for k in range(nz - 1):
         slot = kvg.at[1 - t, lax.rem(z + 1, nz)]
         remote(slot, slot, kp_send.at[k], kp_recv.at[k], partner).wait_recv()
@@ -573,15 +608,11 @@
     latent_heads = jnp.concatenate(outs, axis=0)
 
     own_c.wait()
-    for k, owner, upper in (
-        (2, lax.rem(x + nx - 1, nx), 1),
-        (3, lax.rem(x + 1, nx), 0),
-        (4, lax.rem(x + 2, nx), 0),
-        (5, lax.rem(x + 2, nx), 1),
-    ):
-        remote(
-            w_part(owner, upper), w_part(owner, upper), w_send.at[k], w_recv.at[k], east
-        ).wait_recv()
+    arrived(0, half, behind)
+    arrived(1, 0, ahead)
+    for k, where in enumerate((west, east)):
+        held = w_part(lax.rem(x + 2, nx), k)
+        remote(held, held, v_send.at[k], v_recv.at[k], where).wait_recv()
     for sl in range(2):
         for xl in range(nx):
             slot = homed.at[sl, xl]
@@ -613,6 +644,15 @@
         return carry
 
     lax.fori_loop(0, reach_r, drain, 0)
+
+    def drain_columns(slot, carry):
+        for k, where in enumerate((east, west)):
+            remote(
+                wz.at[slot], wo.at[slot, x], w_send.at[k, slot], w_recv.at[k, slot], where
+            ).wait_send()
+        return carry
+
+    lax.fori_loop(0, nz, drain_columns, 0)
 
     @pl.when(t == 0)
     def _():
@@ -671,7 +711,8 @@
             *pair(half),
             *pair(half - 1),
             *pair(nz - 1),
-            *pair(6),
+            *pair(2, nz),
+            *pair(2),
             *pair(1),
             dma((half,)),
             dma((2, nx)),

time: 129 us -> 128 us (level)
  no operation moved by 1% of the time
where the time goes in v5:
time: 128 us
  Pallas kernels  124 us (97%)
  local copies, waits for them, and re-layouts  2.86 us (2%)
  other arithmetic  1.32 us (1%)
    pallas_call x1, Pallas kernels, layer(): pl.pallas_call(functools.partial(layer_kernel, nz, nx), out_shape=jax.Sha...  124 us

profile of v5, /device:TPU:33, one launch (start us, length us, event | category | flops | bytes accessed | tf_op | source)
XLA Modules:
  0.0 127.9 jit_solution(10379070548554331307)
XLA Ops:
  0.0 0.0 copy-start
  0.0 0.8 constant_dynamic-slice_fusion
  0.8 0.1 copy.27
  0.9 0.0 copy-done
  0.9 0.0 copy-start.2
  0.9 0.1 constant_dynamic-slice_fusion.2
  1.0 0.0 copy-start.1
  1.0 0.1 copy.25
  1.1 0.1 copy.26
  1.2 0.7 fusion.4.small_ref
  1.9 0.0 copy-done.2
  1.9 0.0 copy-done.1
  1.9 0.6 maximum_bitcast_fusion.wt_ref
  2.5 123.7 %layer.1 = bf16[128,1024]{1,0:T(8,128)(2,1)} custom-call(bf16[2,64,2048]{2,1,0:T(8,128)(2,1)} %tok_ref.1, f32[1,2048]{1,0:T(1,128)} %bitcast.9, bf16[32,512]{1,0:T(8,128)(2,1)} %wq_ref.1, bf16[32,512]{1,0:T(8,128)(2,1)} %wk_ref.1, bf16[32,512]{1,0:T(8,128)(2,1)} %wv_ref.1, bf16[32,512]{1,0:T(8,128)(2,1)} %qd_ref.1, bf16[32,256]{1,0:T(8,128)(2,1)} %kvd_ref.1, ...), custom_call_target="tpu_custom_call" | custom-call | tf_op jit(solution)/shard_map/layer/pallas_call | solution.py:675
  126.2 1.7 %copy.29 = bf16[2,64,1024]{2,1,0:T(8,128)(2,1)} copy(bf16[2,64,1024]{2,1,0:T(8,128)(2,1)} %bitcast.8) | data formatting | bytes 524288
Async XLA Ops:
  0.0 0.9 copy-start
  0.9 0.9 copy-start.2
  1.0 0.9 copy-start.1

commit v6 on v5

--- a/solution.py
+++ b/solution.py
@@ -63,7 +63,7 @@
 
 def layer_kernel(
     nz, nx, tok_ref, pre_ref, wq_ref, wk_ref, wv_ref, qd_ref, kvd_ref, small_ref, rate_ref, wt_ref,
-    qgain_ref, kvgain_ref, qup_ref, lup_ref, far_ref, near_ref, dgain_ref, post_ref, out_ref,
+    qgain_ref, kvgain_ref, qup_ref, lup_ref, far_ref, near_ref, dgain_ref, out_ref,
     toks, normed, ws, wz, side, proj, place, blocks, lines_out, latents,
     dr, gr, lr, kvg, wo, homed, ready, state_out, state_in, part_out, part_in,
     loc_sem, wx_send, wx_recv, tok_send, tok_recv, fwd_send, fwd_recv, r_send, r_recv, l_send, l_recv,
@@ -253,8 +253,16 @@
                 go_left(step + 1, part, from_right).start()
 
     def ring(step, carry):
+        weights_step(step)
         columns_step(step)
+        return carry
+
+    def last_weights(step, carry):
         weights_step(step)
+        return carry
+
+    def last_columns(step, carry):
+        columns_step(step)
         return carry
 
     columns_on(z)
@@ -292,7 +300,7 @@
     proj[...] = product(z + 0)
     lax.fori_loop(0, reach_l, gather_product, 0)
     lax.fori_loop(reach_l + 1, 2 * reach_l + 1, gather_product, 0)
-    lax.fori_loop(reach_r - 1, reach_r, ring, 0)
+    lax.fori_loop(reach_r - 1, reach_r, last_weights, 0)
     proj[...] += product(lax.rem(z + reach_r, nz))
 
     for o in range(nx):
@@ -342,6 +350,7 @@
 
     for i in range(half):
         send_lane(i)
+    lax.fori_loop(reach_r - 1, reach_r, last_columns, 0)
 
     for k, (dx, dt, fx, to, back) in enumerate(near):
         slot = lr.at[2 * back + to]
@@ -628,7 +637,7 @@
     whole = part_out[...].astype(F32) + part_in[...].astype(F32)
     scale = lax.rsqrt(jnp.mean(whole * whole, axis=-1, keepdims=True) + NORM_EPS)
     own_half = jnp.where(t == 0, whole[:, : width // 2], whole[:, width // 2 :])
-    out_ref[...] = (own_half * scale * post_ref[...]).astype(BF16)
+    out_ref[...] = own_half * scale
 
     for copy in started:
         copy.wait_send()
@@ -674,7 +683,7 @@
     specs[8] = pl.BlockSpec(memory_space=pltpu.SMEM)
     return pl.pallas_call(
         functools.partial(layer_kernel, nz, nx),
-        out_shape=jax.ShapeDtypeStruct((rows, width // 2), BF16),
+        out_shape=jax.ShapeDtypeStruct((rows, width // 2), F32),
         in_specs=specs,
         out_specs=pl.BlockSpec(memory_space=VM),
         scratch_shapes=[
@@ -789,8 +798,8 @@
         jnp.asarray(far),
         jnp.asarray(near),
         delta_gain[None],
-        post_gain[None],
     )
+    result = (result * post_gain[None]).astype(BF16)
     return result.reshape(seq_count, token_count, result.shape[1])
 
 

time: 128 us -> 129 us (level)
  other arithmetic: 1.32 us -> 3.11 us
  local copies, waits for them, and re-layouts: 2.86 us -> 1.2 us
    convert_element_type x0 -> x1, other arithmetic: none -> 1.79 us  [local(): result = (result * post_gain[None]).astype(BF16)]
    unnamed x10 -> x11, local copies, waits for them, and re-layouts: 1.98 us -> 0.31 us
where the time goes in v6:
time: 129 us
  Pallas kernels  125 us (97%)
  other arithmetic  3.11 us (2%)
    pallas_call x1, Pallas kernels, layer(): pl.pallas_call(functools.partial(layer_kernel, nz, nx), out_shape=jax.Sha...  125 us

profile of v6, /device:TPU:33, one launch (start us, length us, event | category | flops | bytes accessed | tf_op | source)
XLA Modules:
  0.0 128.9 jit_solution(287118871052777120)
XLA Ops:
  0.0 0.0 copy-start
  0.0 0.8 constant_dynamic-slice_fusion
  0.8 0.1 copy.27
  0.9 0.0 copy-done
  0.9 0.0 copy-start.2
  0.9 0.1 constant_dynamic-slice_fusion.2
  1.0 0.0 copy-start.1
  1.0 0.1 copy.25
  1.1 0.1 copy.26
  1.2 0.7 fusion.4.small_ref
  1.9 0.0 copy-done.2
  1.9 0.0 copy-done.1
  1.9 0.6 maximum_bitcast_fusion.wt_ref
  2.5 0.0 copy-start.3
  2.5 124.6 %layer.1 = f32[128,1024]{1,0:T(8,128)} custom-call(bf16[2,64,2048]{2,1,0:T(8,128)(2,1)} %tok_ref.1, f32[1,2048]{1,0:T(1,128)} %bitcast.7, bf16[32,512]{1,0:T(8,128)(2,1)} %wq_ref.1, bf16[32,512]{1,0:T(8,128)(2,1)} %wk_ref.1, bf16[32,512]{1,0:T(8,128)(2,1)} %wv_ref.1, bf16[32,512]{1,0:T(8,128)(2,1)} %qd_ref.1, bf16[32,256]{1,0:T(8,128)(2,1)} %kvd_ref.1, ...), custom_call_target="tpu_custom_call" | custom-call | tf_op jit(solution)/shard_map/layer/pallas_call | solution.py:684
  127.1 0.0 copy-done.3
  127.2 1.8 %multiply_convert_fusion = bf16[128,1024]{1,0:T(8,128)(2,1)} fusion(f32[128,1024]{1,0:T(8,128)} %layer.1, f32[1024]{0:T(1024)S(1)} %copy-done.3), kind=kLoop, calls=%fused_computation | loop fusion | flops 262144 | bytes 790528 | tf_op jit(solution)/shard_map/convert_element_type | solution.py:802
Async XLA Ops:
  0.0 0.9 copy-start
  0.9 0.9 copy-start.2
  1.0 0.9 copy-start.1
  2.5 124.6 %copy-start.3 = (f32[1024]{0:T(1024)S(1)}, f32[1024]{0:T(1024)}, u32[]{:S(2)}) copy-start(f32[1024]{0:T(1024)} %param.39) | copy-start | bytes 12292
